TPU v7x, 32 devices: a whole 2x2x4 slice. The times are simulated.
32 devices in a mesh: sp: 4 (over z), tp: 8 (over y, x, core).
Axes of the slice: x: 2, y: 2, z: 4, core: 2. Of those that a mesh axis runs over, the one named last changes fastest.
Arguments:
- activations: bfloat16 [1024, 2048], P('sp', 'tp'), may hold values from -170 to 170
- norm_gain: float32 [2048], replicated, may hold values from 0.1 to 1.9
- query_weight: bfloat16 [2048, 1536], P(None, 'tp'), may hold values from -0.125 to 0.125
- latent_weight: bfloat16 [2048, 512], P(None, 'tp'), may hold values from -0.125 to 0.125
- rope_key_weight: bfloat16 [2048, 64], replicated, may hold values from -0.125 to 0.125
- latent_gain: float32 [512], replicated, may hold values from 1.5 to 64
- expand_weight: bfloat16 [512, 2048], P(None, 'tp'), may hold values from -0.25 to 0.25
- gate_weight: bfloat16 [2048, 1024], P(None, 'tp'), may hold values from -0.125 to 0.125
- pre_weight: bfloat16 [2048, 1024], P(None, 'tp'), may hold values from -0.125 to 0.125
- value_weight: bfloat16 [2048, 1024], P(None, 'tp'), may hold values from -0.125 to 0.125
- conv_kernel: bfloat16 [3, 1024], P(None, 'tp'), may hold values from -3.5 to 3.5
- output_attend: bfloat16 [1024, 2048], P('tp'), may hold values from -0.1875 to 0.1875
- output_conv: bfloat16 [1024, 2048], P('tp'), may hold values from -0.125 to 0.125
Outputs:
- mixed: bfloat16 [1024, 2048], P(('sp', 'tp'))
- log_weight_sum: float32 [8, 1024], P('tp', 'sp')
All inputs are finite; a program needn't handle non-finite values.
Results may differ from a plain program's by a relative error of at most 0.035.
The roundings to bfloat16 on the way count: a program that leaves them out, or rounds other values in their place, can miss the bound.
Values may be sent and summed in bfloat16 or wider, within the bound.
No kernel may reach another device: no remote copies, remote signals or barrier semaphores. Data moves between devices by JAX's collectives and lax.ppermute only.
A program may use at most 128 MiB of HBM per device.

v0:
```python
import math

import jax
import jax.numpy as jnp
from jax import lax
from jax.sharding import PartitionSpec as P

D = 2048
NOPE = 128
ROPE = 64
VDIM = 128
GRID_W = 64


EPSILON = 1e-06
ROPE_BASE = 10000.0


def with_halo(array, sides, width):
    for axis, dim in sides:
        peers, length = (lax.axis_size(axis), array.shape[dim])
        up = [(i, (i + 1) % peers) for i in range(peers - 1)]
        down = [(j, i) for i, j in up]
        last = lax.slice_in_dim(array, length - width, length, axis=dim)
        leading = lax.slice_in_dim(array, 0, width, axis=dim)
        before = lax.ppermute(last, axis, up)
        after = lax.ppermute(leading, axis, down)
        array = jnp.concatenate([before, array, after], axis=dim)
    return array


def rotate(inputs, grid_rows, grid_cols):
    quarter = inputs.shape[-1] // 4
    inverse = ROPE_BASE ** (-jnp.arange(quarter, dtype=jnp.float32) / quarter)
    row_angle = (grid_rows[:, None] * inverse)[:, None, :]
    col_angle = (grid_cols[:, None] * inverse)[:, None, :]
    part_one = inputs[..., :quarter]
    part_two = inputs[..., quarter : 2 * quarter]
    part_three = inputs[..., 2 * quarter : 3 * quarter]
    part_four = inputs[..., 3 * quarter :]
    return jnp.concatenate(
        [
            part_one * jnp.cos(row_angle) - part_two * jnp.sin(row_angle),
            part_one * jnp.sin(row_angle) + part_two * jnp.cos(row_angle),
            part_three * jnp.cos(col_angle) - part_four * jnp.sin(col_angle),
            part_three * jnp.sin(col_angle) + part_four * jnp.cos(col_angle),
        ],
        axis=-1,
    )


def conv_branch(gate_proj, pre_proj, value_proj, conv_kernel):
    pre_mix = (pre_proj * value_proj).astype(jnp.bfloat16)
    padded = with_halo(pre_mix, (("sp", 0),), 1).astype(jnp.float32)
    kernel = conv_kernel.astype(jnp.float32)
    convolved = kernel[0] * padded[:-2] + kernel[1] * padded[1:-1] + kernel[2] * padded[2:]
    return (gate_proj * convolved).astype(jnp.bfloat16)


def body(
    activations,
    norm_gain,
    query_weight,
    latent_weight,
    rope_key_weight,
    latent_gain,
    expand_weight,
    gate_weight,
    pre_weight,
    value_weight,
    conv_kernel,
    output_attend,
    output_conv,
):
    tokens_here = activations.shape[0]
    query_cols = query_weight.shape[1]
    heads_here = query_cols // (NOPE + ROPE)
    latent_cols = latent_weight.shape[1]
    channels = gate_weight.shape[1]
    joined = jnp.concatenate(
        [query_weight, latent_weight, rope_key_weight, gate_weight, pre_weight, value_weight],
        axis=1,
    )
    inputs_f32 = activations.astype(jnp.float32)
    squares = lax.psum(jnp.sum(inputs_f32 * inputs_f32, axis=1, keepdims=True), "tp")
    partial_squares = jnp.zeros((tokens_here, 1), jnp.float32)
    piece_f32 = lax.all_gather(activations, "tp", axis=1, tiled=True).astype(jnp.float32)
    scaled = (piece_f32 * norm_gain).astype(jnp.bfloat16)
    running = jnp.dot(scaled, joined, preferred_element_type=jnp.float32)
    running, folded_squares = (running, partial_squares)
    inv_rms = lax.rsqrt(squares / D + EPSILON)
    projected = running * inv_rms
    latent_end = query_cols + latent_cols
    rope_end = latent_end + ROPE
    query_proj = projected[:, :query_cols]
    latent_proj = projected[:, query_cols:latent_end]
    rope_proj = projected[:, latent_end:rope_end]
    gate_proj = projected[:, rope_end : rope_end + channels]
    pre_proj = projected[:, rope_end + channels : rope_end + 2 * channels]
    value_proj = projected[:, rope_end + 2 * channels :]
    positions = lax.axis_index("sp") * tokens_here + jnp.arange(tokens_here, dtype=jnp.int32)
    grid_rows = (positions // GRID_W).astype(jnp.float32)
    grid_cols = (positions % GRID_W).astype(jnp.float32)
    query = query_proj.reshape(tokens_here, heads_here, NOPE + ROPE)
    query = jnp.concatenate(
        [query[..., :NOPE], rotate(query[..., NOPE:], grid_rows, grid_cols)], axis=-1
    )
    query = (query * (NOPE + ROPE) ** (-0.5)).astype(jnp.bfloat16)
    query_nope = query[..., :NOPE]
    query_rope = query[..., NOPE:]
    gathered = lax.all_gather(latent_proj.astype(jnp.bfloat16), "tp", axis=1, tiled=True).astype(
        jnp.float32
    )
    latent = (
        gathered
        * lax.rsqrt(jnp.mean(gathered * gathered, axis=1, keepdims=True) + EPSILON)
        * latent_gain
    ).astype(jnp.bfloat16)
    expanded = jnp.dot(latent, expand_weight, preferred_element_type=jnp.float32).astype(
        jnp.bfloat16
    )
    rope_key = rotate(rope_proj[:, None, :], grid_rows, grid_cols)[:, 0].astype(jnp.bfloat16)
    starting = (
        jnp.full((heads_here, tokens_here), -jnp.inf, jnp.float32),
        jnp.zeros((heads_here, tokens_here), jnp.float32),
        jnp.zeros((tokens_here, heads_here, VDIM), jnp.float32),
    )
    key_piece = lax.all_gather(expanded, "sp", axis=0, tiled=True)
    rope_piece = lax.all_gather(rope_key, "sp", axis=0, tiled=True)
    piece_rows = key_piece.shape[0]
    key_block = math.gcd(piece_rows, 1024)
    split_heads = key_piece.reshape(piece_rows, heads_here, NOPE + VDIM)

    def one_block(turn_index, state):
        row_max, row_sum, running_out = state
        offset = turn_index * key_block
        block_keys = lax.dynamic_slice_in_dim(split_heads, offset, key_block, 0)
        block_rope = lax.dynamic_slice_in_dim(rope_piece, offset, key_block, 0)
        scores = jnp.einsum(
            "thd,jhd->htj", query_nope, block_keys[..., :NOPE], preferred_element_type=jnp.float32
        )
        scores = scores + jnp.einsum(
            "thd,jd->htj", query_rope, block_rope, preferred_element_type=jnp.float32
        )
        new_max = jnp.maximum(row_max, jnp.max(scores, axis=-1))
        rescale = jnp.exp(row_max - new_max)
        weights = jnp.exp(scores - new_max[..., None])
        row_sum = row_sum * rescale + jnp.sum(weights, axis=-1)
        running_out = running_out * rescale.T[..., None] + jnp.einsum(
            "htj,jhd->thd",
            weights.astype(jnp.bfloat16),
            block_keys[..., NOPE:],
            preferred_element_type=jnp.float32,
        )
        return (new_max, row_sum, running_out)

    row_max, row_sum, running_out = lax.fori_loop(0, piece_rows // key_block, one_block, starting)
    attended = (
        (running_out / row_sum.T[..., None])
        .astype(jnp.bfloat16)
        .reshape(tokens_here, heads_here * VDIM)
    )
    log_weight_sum = row_max + jnp.log(row_sum)
    conv_mixed = conv_branch(gate_proj, pre_proj, value_proj, conv_kernel)
    mixed = lax.psum_scatter(
        (
            jnp.dot(attended, output_attend, preferred_element_type=jnp.float32)
            + jnp.dot(conv_mixed, output_conv, preferred_element_type=jnp.float32)
        ).astype(jnp.bfloat16),
        "tp",
        scatter_dimension=0,
        tiled=True,
    )
    return (mixed, log_weight_sum)


def solution(mesh):
    return jax.shard_map(
        body,
        mesh=mesh,
        in_specs=(
            P("sp", "tp"),
            P(),
            P(None, "tp"),
            P(None, "tp"),
            P(),
            P(),
            P(None, "tp"),
            P(None, "tp"),
            P(None, "tp"),
            P(None, "tp"),
            P(None, "tp"),
            P("tp", None),
            P("tp", None),
        ),
        out_specs=(P(("sp", "tp"), None), P("tp", "sp")),
        check_vma=False,
    )
```

profile of v0, /device:TPU:0, one launch (start us, length us, event | category | flops | bytes accessed | tf_op | source)
XLA Modules:
  0.0 135.6 jit_solution(17453811287171782455)
XLA Ops:
  7.3 0.7 all-gather.3.cloned.1.call-update
  8.0 1.0 multiply_reduce_fusion
  9.0 1.2 copy.19
  10.3 1.3 copy.20
  11.5 1.2 copy.21
  12.8 15.2 %psum.7 = f32[256,1]{0,1:T(1,128)S(1)} all-reduce(f32[256,1]{0,1:T(1,128)S(1)} %bitcast.73), channel_id=1, replica_groups=mesh['sp'=4,'tp'=8] {'tp'}, use_global_device_ids=true, to_apply=%region_1.0 | all-reduce | flops 256 | bytes 2048 | tf_op jit(solution)/shard_map/psum | solution.py:85
  28.0 0.6 slice_bitcast_fusion.13
  28.6 0.9 constant_dynamic-update-slice_fusion.5
  29.6 0.7 constant_dynamic-update-slice_fusion.4
  30.3 0.7 constant_dynamic-update-slice_fusion.3
  31.0 0.8 constant_dynamic-update-slice_fusion.2
  31.8 0.9 constant_dynamic-update-slice_fusion.1
  32.7 0.8 constant_dynamic-update-slice_fusion
  33.5 2.7 %all-gather.3.cloned.1.call-done = bf16[256,2048]{1,0:T(8,128)(2,1)} async-done(((bf16[256,256]{1,0:T(8,128)(2,1)}), bf16[256,2048]{1,0:T(8,128)(2,1)}) %all-gather.3.cloned.1.call-update) | async-done | bytes 1048592 | tf_op jit(solution)/shard_map/all_gather | solution.py:87
  36.2 3.1 %convolution_multiply_fusion = f32[256,704]{0,1:T(8,128)S(1)} fusion(bf16[2048,704]{0,1:T(8,128)(2,1)} %constant_dynamic-update-slice_fusion, bf16[256,2048]{1,0:T(8,128)(2,1)} %all-gather.3.cloned.1.call-done, f32[2048]{0:T(1024)S(1)} %copy-done.7, f32[256]{0:T(256)S(1)} %bitcast.74), kind=kOutput, calls=%fused_computation.6 | convolution fusion | flops 739950592 | bytes 4662272 | tf_op jit(solution)/shard_map/dot_general | solution.py:89
  39.4 0.1 constant_dynamic-update-slice_fusion.9
  39.6 0.1 constant_dynamic-update-slice_fusion.8
  39.7 0.2 fusion.52
  39.9 13.4 %all-gather = bf16[1024,1,64]{0,2,1:T(8,128)(2,1)S(1)} all-gather(bf16[256,1,64]{0,2,1:T(8,128)(2,1)S(1)} %pad_maximum_fusion), channel_id=2, replica_groups=mesh['sp'=4,'tp'=8] {'sp'}, dimensions={0}, use_global_device_ids=true | all-gather | bytes 163840 | tf_op jit(solution)/shard_map/all_gather | solution.py:129
  53.5 9.3 %all_gather.13 = bf16[256,512]{0,1:T(8,128)(2,1)S(1)} all-gather(bf16[256,64]{0,1:T(8,128)(2,1)S(1)} %slice.196), channel_id=1, replica_groups=mesh['sp'=4,'tp'=8] {'tp'}, dimensions={1}, use_global_device_ids=true | all-gather | bytes 294912 | tf_op jit(solution)/shard_map/all_gather | solution.py:111
  62.9 0.4 convolution_convert_fusion
  63.3 16.1 %all_gather.14 = bf16[1024,256]{1,0:T(8,128)(2,1)S(1)} all-gather(bf16[256,256]{1,0:T(8,128)(2,1)S(1)} %convolution_convert_fusion), channel_id=1, replica_groups=mesh['sp'=4,'tp'=8] {'sp'}, dimensions={0}, use_global_device_ids=true | all-gather | bytes 655360 | tf_op jit(solution)/shard_map/all_gather | solution.py:128
  79.4 0.3 convolution_bitcast_fusion.1
  79.7 0.4 fusion.66
  80.2 0.3 fusion.7
  80.5 3.7 %collective-permute-start = (bf16[1,128]{0,1:T(8,128)(2,1)S(1)}, bf16[1,128]{0,1:T(8,128)(2,1)S(1)}, u32[]{:S(2)}, u32[]{:S(2)}) collective-permute-start(bf16[1,128]{0,1:T(8,128)(2,1)S(1)} %get-tuple-element.26), channel_id=1, source_target_pairs={{0,8},{8,16},{16,24},{1,9},{9,17},{17,25},{2,10},{10,18},{18,26},{... | collective-permute-start | bytes 776 | tf_op jit(solution)/shard_map/ppermute | solution.py:26
  84.2 1.3 collective-permute-start.1
  85.5 2.4 %fusion.9 = f32[256,2048]{1,0:T(8,128)} fusion(bf16[128,2048]{1,0:T(8,128)(2,1)S(1)} %copy-done, f32[1,256,1024]{2,1,0:T(8,128)S(1)} %get-tuple-element.44, f32[256]{0:T(256)S(1)} %get-tuple-element.43, bf16[1024,1,256]{2,0,1:T(8,128)(2,1)S(1)} %bitcast.70, f32[256]{0:T(256)S(1)} %get-tuple-element.42, f32[256]{0:T(256)S(1)} %get-tuple-element.41), kind=kOutput, calls=%fused_computation.19 | convolution fusion | flops 201949184 | bytes 3935232 | tf_op jit(solution)/shard_map/dot_general | solution.py:167
  88.0 2.1 %collective-permute-done.1 = bf16[1,128]{0,1:T(8,128)(2,1)S(1)} collective-permute-done((bf16[1,128]{0,1:T(8,128)(2,1)S(1)}, bf16[1,128]{0,1:T(8,128)(2,1)S(1)}, u32[]{:S(2)}, u32[]{:S(2)}) %collective-permute-start.1) | collective-permute-done | bytes 288 | tf_op jit(solution)/shard_map/ppermute | solution.py:27
  90.2 3.2 %fusion = bf16[256,2048]{1,0:T(8,128)(2,1)} fusion(f32[256,2048]{1,0:T(8,128)} %fusion.9, bf16[128,2048]{1,0:T(8,128)(2,1)S(1)} %copy-done.2, f32[258,128]{0,1:T(8,128)S(1)} %maximum_convert_fusion, f32[256,704]{0,1:T(8,128)S(1)} %convolution_multiply_fusion, f32[128]{0:T(128)} %get-tuple-element.38, f32[128]{0:T(128)} %get-tuple-element.39, ...), kind=kOutput, calls=%fused_computation.1 | convolution fusion | flops 135495680 | bytes 4195840 | tf_op jit(solution)/shard_map/dot_general | solution.py:168
  93.4 0.6 log_add_fusion
  94.0 34.8 %reduce-scatter.2.cloned.1.call-done = bf16[32,2048]{1,0:T(8,128)(2,1)} async-done(((bf16[256,2048]{1,0:T(8,128)(2,1)}), bf16[32,2048]{1,0:T(8,128)(2,1)}) %reduce-scatter.2.cloned.1.call-update) | async-done | bytes 131088 | tf_op jit(solution)/shard_map/reduce_scatter | solution.py:165
  (39 shorter events, 0.7 us)
Async XLA Ops:
  7.2 78.4 %copy-start = (bf16[128,2048]{1,0:T(8,128)(2,1)S(1)}, bf16[128,2048]{1,0:T(8,128)(2,1)}, u32[]{:S(2)}) copy-start(bf16[128,2048]{1,0:T(8,128)(2,1)} %param.24) | copy-start | bytes 1572868
  7.2 20.8 %copy-start.5 = (bf16[3,128]{1,0:T(4,128)(2,1)S(1)}, bf16[3,128]{1,0:T(4,128)(2,1)}, u32[]{:S(2)}) copy-start(bf16[3,128]{1,0:T(4,128)(2,1)} %param.23) | copy-start | bytes 2308
  7.2 21.4 %copy-start.1 = (bf16[2048,192]{0,1:T(8,128)(2,1)S(1)}, bf16[2048,192]{0,1:T(8,128)(2,1)}, u32[]{:S(2)}) copy-start(bf16[2048,192]{0,1:T(8,128)(2,1)} %param.15) | copy-start | bytes 2359300
  7.2 22.3 %copy-start.3 = (bf16[2048,64]{0,1:T(8,128)(2,1)S(1)}, bf16[2048,64]{0,1:T(8,128)(2,1)}, u32[]{:S(2)}) copy-start(bf16[2048,64]{0,1:T(8,128)(2,1)} %param.16) | copy-start | bytes 786436
  7.2 23.1 %copy-start.4 = (bf16[2048,64]{0,1:T(8,128)(2,1)S(1)}, bf16[2048,64]{0,1:T(8,128)(2,1)}, u32[]{:S(2)}) copy-start(bf16[2048,64]{0,1:T(8,128)(2,1)} %param.17) | copy-start | bytes 786436
  7.2 29.0 %all-gather.3.cloned.1.call-start = ((), (), s32[]{:S(2)}) async-start(), calls=%async_computation.1 | async-start | bytes 1179648 | tf_op jit(solution)/shard_map/all_gather | solution.py:87
  8.0 120.8 %reduce-scatter.2.cloned.1.call-start = ((), (), s32[]{:S(2)}) async-start(), calls=%async_computation.2 | async-start | bytes 1179648 | tf_op jit(solution)/shard_map/reduce_scatter | solution.py:165
  28.6 7.6 %copy-start.7 = (f32[2048]{0:T(1024)S(1)}, f32[2048]{0:T(1024)}, u32[]{:S(2)}) copy-start(f32[2048]{0:T(1024)} %param.14) | copy-start | bytes 24580
  36.2 26.7 %copy-start.6 = (bf16[512,256]{1,0:T(8,128)(2,1)S(1)}, bf16[512,256]{1,0:T(8,128)(2,1)}, u32[]{:S(2)}) copy-start(bf16[512,256]{1,0:T(8,128)(2,1)} %param.19) | copy-start | bytes 786436
  36.2 26.7 %copy-start.8 = (f32[512]{0:T(512)S(1)}, f32[512]{0:T(512)}, u32[]{:S(2)}) copy-start(f32[512]{0:T(512)} %param.18) | copy-start | bytes 6148
  80.1 10.0 %copy-start.2 = (bf16[128,2048]{1,0:T(8,128)(2,1)S(1)}, bf16[128,2048]{1,0:T(8,128)(2,1)}, u32[]{:S(2)}) copy-start(bf16[128,2048]{1,0:T(8,128)(2,1)} %param.25) | copy-start | bytes 1572868
  80.5 7.4 %collective-permute-start = (bf16[1,128]{0,1:T(8,128)(2,1)S(1)}, bf16[1,128]{0,1:T(8,128)(2,1)S(1)}, u32[]{:S(2)}, u32[]{:S(2)}) collective-permute-start(bf16[1,128]{0,1:T(8,128)(2,1)S(1)} %get-tuple-element.26), channel_id=1, source_target_pairs={{0,8},{8,16},{16,24},{1,9},{9,17},{17,25},{2,10},{10,18},{18,26},{... | collective-permute-start | bytes 776 | tf_op jit(solution)/shard_map/ppermute | solution.py:26
  84.2 5.8 %collective-permute-start.1 = (bf16[1,128]{0,1:T(8,128)(2,1)S(1)}, bf16[1,128]{0,1:T(8,128)(2,1)S(1)}, u32[]{:S(2)}, u32[]{:S(2)}) collective-permute-start(bf16[1,128]{0,1:T(8,128)(2,1)S(1)} %get-tuple-element.36), channel_id=1, source_target_pairs={{8,0},{16,8},{24,16},{9,1},{17,9},{25,17},{10,2},{18,10},{26,18},{... | collective-permute-start | bytes 776 | tf_op jit(solution)/shard_map/ppermute | solution.py:27
Sparse Core Ops, SparseCore 0:
  9.9 26.2 all-gather.2
  93.5 35.1 reduce-scatter.1
where the time goes:
time: 136 us
  blocking collectives  53.9 us (40%)
  waiting for transfers between devices  40.2 us (30%)
  between operations  14.3 us (11%)
  matrix products  9.9 us (7%)
  local copies, waits for them, and re-layouts  9.39 us (7%)
  starting transfers between devices  5.04 us (4%)
  other arithmetic  2.83 us (2%)
    reduce_scatter x1, waiting for transfers between devices, body(): lax.psum_scatter((jnp.dot(attended, output_attend, preferred_element_type...  34.8 us
    all_gather x1, blocking collectives, body(): key_piece = lax.all_gather(expanded, 'sp', axis=0, tiled=True)  16.1 us
    psum x1, blocking collectives, body(): lax.psum(jnp.sum(inputs_f32 * inputs_f32, axis=1, keepdims=True), 'tp')  15.2 us
    all_gather x1, blocking collectives, body(): rope_piece = lax.all_gather(rope_key, 'sp', axis=0, tiled=True)  13.4 us
    all_gather x1, blocking collectives, body(): lax.all_gather(latent_proj.astype(jnp.bfloat16), 'tp', axis=1, tiled=True)  9.26 us
    unnamed x27, local copies, waits for them, and re-layouts  7.86 us
    ppermute x1, starting transfers between devices, with_halo(): before = lax.ppermute(last, axis, up)  3.67 us
    dot_general x1, matrix products, body(): jnp.dot(conv_mixed, output_conv, preferred_element_type=jnp.float32)  3.22 us
  transfers between devices with their start and end apart: 4, of which 3 were waited for; matrix products, arithmetic and copies ran while one was open for 10% of the time, Pallas kernels for 0%

commit v1 on v0

v1 whole, which is shorter than its diff:
```python
import functools

import jax
import jax.numpy as jnp
from jax import lax
from jax.experimental import pallas as pl
from jax.experimental.pallas import tpu as pltpu
from jax.sharding import PartitionSpec as P

NOPE = 128
ROPE = 64
VDIM = 128
GRID_W = 64
EPSILON = 1e-06
ROPE_BASE = 10000.0
LANES = 128
HALO = 16
F32 = jnp.float32
BF16 = jnp.bfloat16


def swap(array, axis, mask):
    peers = lax.axis_size(axis)
    return lax.ppermute(array, axis, [(i, i ^ mask) for i in range(peers)])


def kernel_call(body, outs, limit, scratch=(), flops=0, nbytes=0, name=None):
    whole = pl.BlockSpec(memory_space=pltpu.VMEM)

    def call(*operands):
        return pl.pallas_call(
            body,
            out_shape=[jax.ShapeDtypeStruct(shape, dtype) for shape, dtype in outs],
            in_specs=[whole] * len(operands),
            out_specs=[whole] * len(outs),
            scratch_shapes=list(scratch),
            compiler_params=pltpu.CompilerParams(vmem_limit_bytes=limit),
            cost_estimate=pl.CostEstimate(flops=flops, bytes_accessed=nbytes, transcendentals=0),
            name=name,
        )(*operands)

    return call


def rotation(positions):
    lane = jnp.arange(LANES) % ROPE
    quarter = ROPE // 4
    inverse = ROPE_BASE ** (-(lane % quarter).astype(F32) / quarter)
    rows = (positions // GRID_W).astype(F32)[:, None]
    cols = (positions % GRID_W).astype(F32)[:, None]
    angle = jnp.where(lane < 2 * quarter, rows, cols) * inverse
    sign = jnp.where((lane // quarter) % 2 == 0, -1.0, 1.0).astype(F32)
    return jnp.cos(angle), jnp.sin(angle) * sign


def rotate(values, cosines, sines):
    quarter = ROPE // 4
    lane = lax.broadcasted_iota(jnp.int32, values.shape, 1)
    first = (lane // quarter) % 2 == 0
    ahead = pltpu.roll(values, LANES - quarter, 1)
    behind = pltpu.roll(values, quarter, 1)
    return values * cosines + jnp.where(first, ahead, behind) * sines


def low_lanes(shape):
    return lax.broadcasted_iota(jnp.int32, shape, 1) < ROPE


def project_first(
    even_ref, odd_ref, gain_ref, key_w_ref, mix_w_ref, cos_ref, sin_ref,
    scaled_ref, inv_ref, message_ref, mix_ref, key_ref,
):
    rank = lax.axis_index("tp")
    pairs, tokens, width = even_ref.shape
    half = tokens // 2
    total = jnp.zeros((tokens, LANES), F32)
    for core, ref in ((0, even_ref), (1, odd_ref)):
        for i in range(pairs):
            owner = rank ^ (2 * i + core)
            piece = ref[i].astype(F32)
            squares = piece * piece
            for j in range(width // LANES):
                total = total + squares[:, j * LANES : (j + 1) * LANES]
            gain = gain_ref[pl.ds(owner, 1), :]
            start = pl.multiple_of(owner * width, width)
            scaled_ref[:, pl.ds(start, width)] = (piece * gain).astype(BF16)
    features = 2 * pairs * width
    inv = lax.rsqrt(jnp.sum(total, axis=1, keepdims=True) / features + EPSILON)
    inv_ref[...] = jnp.broadcast_to(inv, inv_ref.shape)
    scaled = scaled_ref[...]
    keys = jnp.dot(scaled, key_w_ref[...], preferred_element_type=F32) * inv
    mixes = jnp.dot(scaled, mix_w_ref[...], preferred_element_type=F32) * inv
    mix = (mixes[:, :LANES] * mixes[:, LANES:]).astype(BF16)
    mix_ref[...] = mix
    latent = keys[:, :LANES]
    low = low_lanes((half, LANES))
    message_ref[:half, :] = jnp.where(low, latent[:half], latent[half:]).astype(BF16)
    key_ref[...] = keys[:, LANES:]
    share = half // (2 * pairs)
    start = pl.multiple_of(rank * share, share)
    turned = []
    for base in (0, half):
        rows = pl.ds(start + base, share)
        turned.append(rotate(key_ref[rows, :], cos_ref[rows, :], sin_ref[rows, :]))
    low = low_lanes((share, LANES))
    message_ref[half : half + share, :] = jnp.where(low, turned[0], turned[1]).astype(BF16)
    row = lax.broadcasted_iota(jnp.int32, (HALO, LANES), 0)
    first = jnp.broadcast_to(mix[:1].astype(F32), (HALO, LANES))
    last = jnp.broadcast_to(mix[tokens - 1 :].astype(F32), (HALO, LANES))
    message_ref[half + share :, :] = jnp.where(row == 0, first, last).astype(BF16)


def project_second(
    scaled_ref, inv_ref, query_w_ref, gate_w_ref, cos_ref, sin_ref, query_ref, gate_ref
):
    scaled = scaled_ref[...]
    inv = inv_ref[...]
    scale = (NOPE + ROPE) ** (-0.5)
    query = jnp.dot(scaled, query_w_ref[...], preferred_element_type=F32)
    gate_ref[...] = jnp.dot(scaled, gate_w_ref[...], preferred_element_type=F32) * inv
    nope = (query[:, :NOPE] * inv * scale).astype(BF16)
    rope = rotate(query[:, NOPE:] * inv, cos_ref[...], sin_ref[...]) * scale
    low = low_lanes(rope.shape)
    query_ref[0, :, :NOPE] = nope
    query_ref[1, :, :NOPE] = nope
    query_ref[0, :, NOPE:] = jnp.where(low, rope, 0.0).astype(BF16)
    query_ref[1, :, NOPE:] = jnp.where(low, 0.0, rope).astype(BF16)


def attend(
    chunk, natural, even_ref, odd_ref, halo_ref, gain_ref, expand_ref, query_ref, gate_ref,
    mix_ref, taps_ref, keep_ref, send_ref, log_ref, latent_ref, rope_ref, both_ref,
):
    rank = lax.axis_index("tp")
    place = lax.axis_index("sp")
    pairs, blocks, _, _ = even_ref.shape
    ranks = 2 * pairs
    tokens = query_ref.shape[1]
    half = tokens // 2
    share = half // ranks
    entries = ranks * ROPE
    low = low_lanes((half, LANES))
    owned = [(rank ^ (2 * i + core), ref, i) for core, ref in ((0, even_ref), (1, odd_ref)) for i in range(pairs)]

    def one_chunk(first, state):
        scores, values = [], []
        for slot in range(chunk):
            block = first + slot
            total = jnp.zeros((half, LANES), F32)
            for owner, ref, i in owned:
                piece = ref[i, block, :half, :].astype(F32)
                total = total + piece * piece
                start = pl.multiple_of(owner * share, share)
                rope_ref[slot, pl.ds(start, share), :] = ref[i, block, half : half + share, :]
            sum_low = jnp.sum(jnp.where(low, total, 0.0), axis=1, keepdims=True)
            sum_high = jnp.sum(jnp.where(low, 0.0, total), axis=1, keepdims=True)
            inv = lax.rsqrt(jnp.where(low, sum_low, sum_high) / entries + EPSILON)
            for owner, ref, i in owned:
                piece = ref[i, block, :half, :].astype(F32)
                start = pl.multiple_of(owner * LANES, LANES)
                latent_ref[slot, :, pl.ds(start, LANES)] = (piece * inv * gain_ref[pl.ds(owner, 1), :]).astype(BF16)
        for slot in range(chunk):
            expanded = jnp.dot(latent_ref[slot], expand_ref[...], preferred_element_type=F32).astype(BF16)
            for side in range(2):
                base = side * (NOPE + VDIM)
                keys = jnp.concatenate([expanded[:, base : base + NOPE], rope_ref[slot]], axis=1)
                values.append(expanded[:, base + NOPE : base + NOPE + VDIM])
                scores.append(
                    lax.dot_general(query_ref[side], keys, (((1,), (1,)), ((), ())), preferred_element_type=F32)
                )
        peak = scores[0]
        for piece in scores[1:]:
            peak = jnp.maximum(peak, piece)
        peak = jnp.max(peak, axis=1, keepdims=True)
        if state is not None:
            peak = jnp.maximum(peak, state[0])
        total = jnp.zeros((tokens, LANES), F32)
        out = jnp.zeros((tokens, VDIM), F32)
        for piece, value in zip(scores, values, strict=True):
            weight = jnp.exp(piece - peak)
            total = total + weight
            out = out + jnp.dot(weight.astype(BF16), value, preferred_element_type=F32)
        total = jnp.sum(total, axis=1, keepdims=True)
        if state is not None:
            rescale = jnp.exp(state[0] - peak)
            total = total + state[1] * rescale
            out = out + state[2] * rescale
        return peak, total, out

    if blocks == chunk:
        peak, total, out = one_chunk(0, None)
    else:
        start = (
            jnp.full((tokens, 1), -jnp.inf, F32),
            jnp.zeros((tokens, 1), F32),
            jnp.zeros((tokens, VDIM), F32),
        )
        peak, total, out = lax.fori_loop(0, blocks // chunk, lambda i, state: one_chunk(i * chunk, state), start)
    both_ref[:, :VDIM] = out / total
    logs = jnp.broadcast_to(peak + jnp.log(total), (tokens, LANES))
    log_ref[...] = jnp.transpose(logs)[:1, :]

    mix = mix_ref[...].astype(F32)
    before_at = jnp.maximum(place - 1, 0)
    after_at = jnp.minimum(place + 1, blocks - 1)
    if not natural:
        before_at, after_at = before_at ^ place, after_at ^ place
    before = jnp.where(place > 0, halo_ref[before_at].astype(F32)[1:2, :], 0.0)
    after = jnp.where(place < blocks - 1, halo_ref[after_at].astype(F32)[0:1, :], 0.0)
    row = lax.broadcasted_iota(jnp.int32, mix.shape, 0)
    earlier = jnp.where(row == 0, before, pltpu.roll(mix, 1, 0))
    later = jnp.where(row == tokens - 1, after, pltpu.roll(mix, tokens - 1, 0))
    taps = taps_ref[...].astype(F32)
    convolved = taps[0:1] * earlier + taps[1:2] * mix + taps[2:3] * later
    both_ref[:, VDIM:] = gate_ref[...] * convolved

    chip, core = rank // 2, rank % 2
    rows = tokens // ranks
    for i in range(pairs):
        base = 2 * (chip ^ i)
        mine = pl.multiple_of((base + core) * rows, rows)
        other = pl.multiple_of((base + 1 - core) * rows, rows)
        keep_ref[i * rows : (i + 1) * rows, :] = both_ref[pl.ds(mine, rows), :].astype(BF16)
        send_ref[i * rows : (i + 1) * rows, :] = both_ref[pl.ds(other, rows), :].astype(BF16)


def output(keep_ref, got_ref, own_w_ref, other_w_ref, first_ref, *rest_refs):
    out = jnp.dot(keep_ref[...], own_w_ref[...], preferred_element_type=F32)
    out = out + jnp.dot(got_ref[...], other_w_ref[...], preferred_element_type=F32)
    rows = first_ref.shape[0]
    first_ref[...] = out[:rows]
    for i, ref in enumerate(rest_refs):
        ref[...] = out[(i + 1) * rows : (i + 2) * rows].astype(BF16)


def body(
    activations,
    norm_gain,
    query_weight,
    latent_weight,
    rope_key_weight,
    latent_gain,
    expand_weight,
    gate_weight,
    pre_weight,
    value_weight,
    conv_kernel,
    output_attend,
    output_conv,
):
    ranks = lax.axis_size("tp")
    places = lax.axis_size("sp")
    pairs = ranks // 2
    tokens, width = activations.shape
    features = ranks * width
    half = tokens // 2
    share = half // ranks
    rows = tokens // ranks
    channels = gate_weight.shape[1]

    gathered = [activations] + [swap(activations, "tp", 2 * i) for i in range(1, pairs)]
    even = jnp.stack(gathered)
    odd = swap(even, "tp", 1)
    own_w = jnp.concatenate([output_attend, output_conv], axis=0)
    other_w = swap(own_w, "tp", 1)

    key_w = jnp.concatenate([latent_weight, latent_weight, rope_key_weight, rope_key_weight], axis=1)
    mix_w = jnp.concatenate([pre_weight, value_weight], axis=1)
    query_w = jnp.concatenate([query_weight, query_weight[:, NOPE:]], axis=1)
    parts = expand_weight.reshape(ranks, 1, ROPE, 1, NOPE + VDIM)
    eye = jnp.eye(2, dtype=BF16).reshape(1, 2, 1, 2, 1)
    expand_w = (parts * eye).reshape(ranks * LANES, 2 * (NOPE + VDIM))
    gain = norm_gain.reshape(ranks, width)
    lat_gain = jnp.tile(latent_gain.reshape(ranks, ROPE), (1, 2))
    positions = lax.axis_index("sp") * tokens + jnp.arange(tokens, dtype=jnp.int32)
    cosines, sines = rotation(positions)

    message_rows = half + share + HALO
    scaled, inv, message, mix = kernel_call(
        project_first,
        [((tokens, features), BF16), ((tokens, LANES), F32), ((message_rows, LANES), BF16), ((tokens, channels), BF16)],
        12 << 20,
        scratch=[pltpu.VMEM((tokens, LANES), F32)],
        flops=2 * tokens * features * 4 * LANES,
        nbytes=4 * tokens * features,
        name="project_first",
    )(even, odd, gain, key_w, mix_w, cosines, sines)

    small = places <= 8 and places & (places - 1) == 0
    if small:
        around = [message] + [swap(message, "sp", i) for i in range(1, places)]
        around = jnp.stack(around)
    else:
        around = lax.all_gather(message, "sp", axis=0)
    query, gate = kernel_call(
        project_second,
        [((2, tokens, NOPE + LANES), BF16), ((tokens, channels), F32)],
        12 << 20,
        flops=2 * tokens * features * 3 * LANES,
        nbytes=4 * tokens * features,
        name="project_second",
    )(scaled, inv, query_w, gate_weight, cosines, sines)
    halo = around[:, half + share :, :]
    parts = around[:, : half + share, :]
    chip_even = jnp.stack([parts] + [swap(parts, "tp", 2 * i) for i in range(1, pairs)])
    chip_odd = swap(chip_even, "tp", 1)

    chunk = places if small else 4
    keep, send, logs = kernel_call(
        functools.partial(attend, chunk, not small),
        [((tokens // 2, VDIM + channels), BF16), ((tokens // 2, VDIM + channels), BF16), ((1, tokens), F32)],
        (16 << 20) if small else (60 << 20),
        scratch=[
            pltpu.VMEM((chunk, half, ranks * LANES), BF16),
            pltpu.VMEM((chunk, half, LANES), BF16),
            pltpu.VMEM((tokens, VDIM + channels), F32),
        ],
        flops=1 << 30,
        nbytes=1 << 22,
        name="attend",
    )(chip_even, chip_odd, halo, lat_gain, expand_w, query, gate, mix, conv_kernel)

    got = swap(send, "tp", 1)
    outs = kernel_call(
        output,
        [((rows, features), F32)] + [((rows, features), BF16)] * (pairs - 1),
        12 << 20,
        flops=1 << 28,
        nbytes=1 << 22,
        name="output",
    )(keep, got, own_w, other_w)
    total = outs[0]
    for i in range(1, pairs):
        total = total + swap(outs[i], "tp", 2 * i).astype(F32)
    return total.astype(BF16), logs


def solution(mesh):
    return jax.shard_map(
        body,
        mesh=mesh,
        in_specs=(
            P("sp", "tp"),
            P(),
            P(None, "tp"),
            P(None, "tp"),
            P(),
            P(),
            P(None, "tp"),
            P(None, "tp"),
            P(None, "tp"),
            P(None, "tp"),
            P(None, "tp"),
            P("tp", None),
            P("tp", None),
        ),
        out_specs=(P(("sp", "tp"), None), P("tp", "sp")),
        check_vma=False,
    )
```

time: 136 us -> 61.8 us (0.45)
  blocking collectives: 53.9 us -> 0 us
  waiting for transfers between devices: 40.2 us -> 20.2 us
  between operations: 14.3 us -> 0.98 us
  starting transfers between devices: 5.04 us -> 16.7 us
  matrix products: 9.9 us -> 0 us
  Pallas kernels: 0 us -> 6.75 us
  other arithmetic: 2.83 us -> 8.81 us
    all_gather x3 -> x0, blocking collectives: 38.8 us -> none  [the longest x1 16.1 us: body(): key_piece = lax.all_gather(expanded, 'sp', axis=0, tiled=True)]
    reduce_scatter x1 -> x0, waiting for transfers between devices: 34.8 us -> none  [body(): lax.psum_scatter((jnp.dot(attended, output_attend, preferred_element_type...]
    ppermute x2 -> x16, waiting for transfers between devices: 2.06 us -> 20.2 us  [swap(): return lax.ppermute(array, axis, [(i, i ^ mask) for i in range(peers)])]
    psum x1 -> x0, blocking collectives: 15.2 us -> none  [body(): lax.psum(jnp.sum(inputs_f32 * inputs_f32, axis=1, keepdims=True), 'tp')]
    ppermute x2 -> x16, starting transfers between devices: 4.97 us -> 16.7 us  [swap(): return lax.ppermute(array, axis, [(i, i ^ mask) for i in range(peers)])]
    dot_general x6 -> x0, matrix products: 9.9 us -> none  [the longest x1 3.22 us: body(): jnp.dot(conv_mixed, output_conv, preferred_element_type=jnp.float32)]
    pallas_call x0 -> x4, Pallas kernels: none -> 6.75 us  [call(): pl.pallas_call(body, out_shape=[jax.ShapeDtypeStruct(shape, dtype) for sh...]
    concatenate x2, other arithmetic: 0.15 us -> 3.61 us  [the longest x1 1.83 us: body(): jnp.concatenate([latent_weight, latent_weight, rope_key_weight, rope_key_...]
  transfers between devices with their start and end apart: 4 -> 16, of which waited for: 3 -> 10; matrix products, arithmetic and copies ran while one was open for 10% -> 22% of each run, Pallas kernels for 0% -> 8%
where the time goes in v1:
time: 61.8 us; the launch traced here: 61.5 us
  waiting for transfers between devices  20.2 us (33%)
  starting transfers between devices  16.7 us (27%)
  other arithmetic  8.81 us (14%)
  local copies, waits for them, and re-layouts  8.06 us (13%)
  Pallas kernels  6.75 us (11%)
  between operations  0.98 us (2%)
    ppermute x16, waiting for transfers between devices, swap(): return lax.ppermute(array, axis, [(i, i ^ mask) for i in range(peers)])  20.2 us
    ppermute x16, starting transfers between devices, swap(): return lax.ppermute(array, axis, [(i, i ^ mask) for i in range(peers)])  16.7 us
    pallas_call x4, Pallas kernels, call(): pl.pallas_call(body, out_shape=[jax.ShapeDtypeStruct(shape, dtype) for sh...  6.75 us
    unnamed x45, local copies, waits for them, and re-layouts  5.19 us
    another operation x1, other arithmetic, body(): jnp.stack([parts] + [swap(parts, 'tp', 2 * i) for i in range(1, pairs)])  1.96 us
    slice x1, local copies, waits for them, and re-layouts, body(): query_w = jnp.concatenate([query_weight, query_weight[:, NOPE:]], axis=1)  1.92 us
    concatenate x1, other arithmetic, body(): jnp.concatenate([latent_weight, latent_weight, rope_key_weight, rope_key_...  1.83 us
    concatenate x1, other arithmetic, body(): query_w = jnp.concatenate([query_weight, query_weight[:, NOPE:]], axis=1)  1.77 us
  transfers between devices with their start and end apart: 16, of which 10 were waited for; matrix products, arithmetic and copies ran while one was open for 22% of the time, Pallas kernels for 8%

profile of v1, /device:TPU:0, one launch (start us, length us, event | category | flops | bytes accessed | tf_op | source)
XLA Modules:
  0.0 61.5 jit_solution(1620881002122999317)
XLA Ops:
  0.6 3.0 %collective-permute-start = (bf16[256,256]{1,0:T(8,128)(2,1)}, bf16[256,256]{1,0:T(8,128)(2,1)S(1)}, u32[]{:S(2)}, u32[]{:S(2)}) collective-permute-start(bf16[256,256]{1,0:T(8,128)(2,1)} %param.13), channel_id=1, source_target_pairs={{0,2},{1,3},{2,0},{3,1},{4,6},{5,7},{6,4},{7,5},{8,10},{9,11},{10,... | collective-permute-start | bytes 393224 | tf_op jit(solution)/shard_map/ppermute | solution.py:24
  3.7 1.5 %collective-permute-start.1 = (bf16[256,256]{1,0:T(8,128)(2,1)}, bf16[256,256]{1,0:T(8,128)(2,1)S(1)}, u32[]{:S(2)}, u32[]{:S(2)}) collective-permute-start(bf16[256,256]{1,0:T(8,128)(2,1)} %param.13), channel_id=1, source_target_pairs={{0,4},{1,5},{2,6},{3,7},{4,0},{5,1},{6,2},{7,3},{8,12},{9,13},{10,... | collective-permute-start | bytes 393224 | tf_op jit(solution)/shard_map/ppermute | solution.py:24
  5.3 2.6 %collective-permute-done = bf16[256,256]{1,0:T(8,128)(2,1)S(1)} collective-permute-done((bf16[256,256]{1,0:T(8,128)(2,1)}, bf16[256,256]{1,0:T(8,128)(2,1)S(1)}, u32[]{:S(2)}, u32[]{:S(2)}) %collective-permute-start) | collective-permute-done | bytes 131104 | tf_op jit(solution)/shard_map/ppermute | solution.py:24
  7.9 3.8 %collective-permute-done.1 = bf16[256,256]{1,0:T(8,128)(2,1)S(1)} collective-permute-done((bf16[256,256]{1,0:T(8,128)(2,1)}, bf16[256,256]{1,0:T(8,128)(2,1)S(1)}, u32[]{:S(2)}, u32[]{:S(2)}) %collective-permute-start.1) | collective-permute-done | bytes 131104 | tf_op jit(solution)/shard_map/ppermute | solution.py:24
  11.7 1.0 %pad_maximum_fusion.4.even_ref = bf16[4,256,256]{2,1,0:T(8,128)(2,1)S(1)} fusion(bf16[1,256,256]{2,1,0:T(8,128)(2,1)S(1)} %bitcast.31, bf16[1,256,256]{2,1,0:T(8,128)(2,1)S(1)} %bitcast.30, bf16[1,256,256]{2,1,0:T(8,128)(2,1)S(1)} %bitcast.29, bf16[1,256,256]{2,1,0:T(8,128)(2,1)} %bitcast.28), kind=kLoop, calls=%fused_computation.4 | loop fusion | flops 786432 | bytes 1048576 | tf_op jit(solution)/shard_map/stack | solution.py:262
  13.9 1.8 %pad_maximum_fusion = (bf16[2048,256]{1,0:T(8,128)(2,1)S(1)}, bf16[2048,256]{1,0:T(8,128)(2,1)S(1)}) fusion(bf16[2048,64]{1,0:T(8,128)(2,1)S(1)} %copy.17, bf16[2048,64]{1,0:T(8,128)(2,1)S(1)} %copy.15, bf16[2048,128]{1,0:T(8,128)(2,1)S(1)} %copy-done.8, bf16[2048,128]{1,0:T(8,128)(2,1)} %param.21), kind=kLoop, calls=%fused_computation | loop fusion | flops 6291456 | bytes 3670016 | tf_op jit(solution)/shard_map/concatenate | solution.py:267
  15.8 1.1 %project_first.1 = (bf16[256,2048]{1,0:T(8,128)(2,1)S(1)}, f32[256,128]{1,0:T(8,128)S(1)}, bf16[160,128]{1,0:T(8,128)(2,1)S(1)}, bf16[256,128]{1,0:T(8,128)(2,1)S(1)}) custom-call(bf16[4,256,256]{2,1,0:T(8,128)(2,1)S(1)} %pad_maximum_fusion.4.even_ref, bf16[4,256,256]{2,1,0:T(8,128)(2,1)S(1)} %collective-permute-done.3.odd_ref, ...), custom_call_target="tpu_custom_call" | custom-call | flops 536870912 | bytes 2097152 | tf_op jit(solution)/shard_map/project_first/pallas_call | solution.py:31
  17.6 1.6 %collective-permute-start.4 = (bf16[160,128]{1,0:T(8,128)(2,1)S(1)}, bf16[160,128]{1,0:T(8,128)(2,1)S(1)}, u32[]{:S(2)}, u32[]{:S(2)}) collective-permute-start(bf16[160,128]{1,0:T(8,128)(2,1)S(1)} %get-tuple-element.15), channel_id=1, source_target_pairs={{0,8},{8,0},{16,24},{24,16},{1,9},{9,1},{17,25},{25,17},{2,10},{10... | collective-permute-start | bytes 122888 | tf_op jit(solution)/shard_map/ppermute | solution.py:24
  19.2 2.6 %collective-permute-start.5 = (bf16[160,128]{1,0:T(8,128)(2,1)S(1)}, bf16[160,128]{1,0:T(8,128)(2,1)S(1)}, u32[]{:S(2)}, u32[]{:S(2)}) collective-permute-start(bf16[160,128]{1,0:T(8,128)(2,1)S(1)} %get-tuple-element.15), channel_id=1, source_target_pairs={{0,16},{8,24},{16,0},{24,8},{1,17},{9,25},{17,1},{25,9},{2,18},{10... | collective-permute-start | bytes 122888 | tf_op jit(solution)/shard_map/ppermute | solution.py:24
  22.0 2.9 %collective-permute-done.5 = bf16[160,128]{1,0:T(8,128)(2,1)S(1)} collective-permute-done((bf16[160,128]{1,0:T(8,128)(2,1)S(1)}, bf16[160,128]{1,0:T(8,128)(2,1)S(1)}, u32[]{:S(2)}, u32[]{:S(2)}) %collective-permute-start.5) | collective-permute-done | bytes 40992 | tf_op jit(solution)/shard_map/ppermute | solution.py:24
  24.9 2.7 %collective-permute-done.6 = bf16[160,128]{1,0:T(8,128)(2,1)S(1)} collective-permute-done((bf16[160,128]{1,0:T(8,128)(2,1)S(1)}, bf16[160,128]{1,0:T(8,128)(2,1)S(1)}, u32[]{:S(2)}, u32[]{:S(2)}) %collective-permute-start.6) | collective-permute-done | bytes 40992 | tf_op jit(solution)/shard_map/ppermute | solution.py:24
  27.6 0.8 %slice_bitcast_fusion = (bf16[1,4,144,128]{3,2,1,0:T(8,128)(2,1)}, bf16[4,144,128]{2,1,0:T(8,128)(2,1)}) fusion(bf16[4,160,128]{2,1,0:T(8,128)(2,1)S(1)} %pad_maximum_fusion.5), kind=kLoop, calls=%fused_computation.41 | loop fusion | bytes 442368 | tf_op jit(solution)/shard_map/stack | solution.py:305
  28.3 1.5 %collective-permute-start.8 = (bf16[4,144,128]{2,1,0:T(8,128)(2,1)}, bf16[4,144,128]{2,1,0:T(8,128)(2,1)}, u32[]{:S(2)}, u32[]{:S(2)}) collective-permute-start(bf16[4,144,128]{2,1,0:T(8,128)(2,1)} %get-tuple-element.29), channel_id=1, source_target_pairs={{0,4},{1,5},{2,6},{3,7},{4,0},{5,1},{6,2},{7,3},{8,12},{9,13},{10,... | collective-permute-start | bytes 442376 | tf_op jit(solution)/shard_map/ppermute | solution.py:24
  29.8 1.2 %collective-permute-start.9 = (bf16[4,144,128]{2,1,0:T(8,128)(2,1)}, bf16[4,144,128]{2,1,0:T(8,128)(2,1)}, u32[]{:S(2)}, u32[]{:S(2)}) collective-permute-start(bf16[4,144,128]{2,1,0:T(8,128)(2,1)} %get-tuple-element.29), channel_id=1, source_target_pairs={{0,6},{1,7},{2,4},{3,5},{4,2},{5,3},{6,0},{7,1},{8,14},{9,15},{10,... | collective-permute-start | bytes 442376 | tf_op jit(solution)/shard_map/ppermute | solution.py:24
  31.0 0.8 %collective-permute-start.7 = (bf16[4,144,128]{2,1,0:T(8,128)(2,1)}, bf16[4,144,128]{2,1,0:T(8,128)(2,1)}, u32[]{:S(2)}, u32[]{:S(2)}) collective-permute-start(bf16[4,144,128]{2,1,0:T(8,128)(2,1)} %get-tuple-element.29), channel_id=1, source_target_pairs={{0,2},{1,3},{2,0},{3,1},{4,6},{5,7},{6,4},{7,5},{8,10},{9,11},{10,... | collective-permute-start | bytes 442376 | tf_op jit(solution)/shard_map/ppermute | solution.py:24
  32.0 2.2 %copy.20 = bf16[2048,192]{1,0:T(8,128)(2,1)} copy(bf16[2048,192]{0,1:T(8,128)(2,1)} %param.15) | data formatting | bytes 1572864 | tf_op args[2]
  34.2 1.9 %slice.13 = bf16[2048,64]{1,0:T(8,128)(2,1)} slice(bf16[2048,192]{1,0:T(8,128)(2,1)} %copy.20), slice={[0:2048], [128:192]} | slice | bytes 524288 | tf_op jit(solution)/shard_map/slice | solution.py:269
  36.1 0.7 %collective-permute-done.9 = bf16[4,144,128]{2,1,0:T(8,128)(2,1)} collective-permute-done((bf16[4,144,128]{2,1,0:T(8,128)(2,1)}, bf16[4,144,128]{2,1,0:T(8,128)(2,1)}, u32[]{:S(2)}, u32[]{:S(2)}) %collective-permute-start.9) | collective-permute-done | bytes 147488 | tf_op jit(solution)/shard_map/ppermute | solution.py:24
  37.6 2.0 %pad_maximum_fusion.3.even_ref = bf16[4,4,144,128]{3,2,1,0:T(8,128)(2,1)} fusion(bf16[1,4,144,128]{3,2,1,0:T(8,128)(2,1)} %bitcast.11, bf16[1,4,144,128]{3,2,1,0:T(8,128)(2,1)} %bitcast.10, bf16[1,4,144,128]{3,2,1,0:T(8,128)(2,1)} %bitcast.9, bf16[1,4,144,128]{3,2,1,0:T(8,128)(2,1)S(1)} %copy-done.5), kind=kLoop, calls=%fused_computation.3 | loop fusion | flops 884736 | bytes 1179648 | tf_op jit(solution)/shard_map/stack | solution.py:305
  39.5 0.9 %broadcast_multiply_fusion = bf16[8,2,64,2,256]{4,3,2,1,0:T(2,128)(2,1)S(1)} fusion(bf16[2,2]{1,0:T(2,128)(2,1)S(1)} %compare_convert_fusion, bf16[8,64,256]{2,1,0:T(8,128)(2,1)S(1)} %bitcast.21), kind=kLoop, calls=%fused_computation.5 | loop fusion | flops 524288 | bytes 1310728 | tf_op jit(solution)/shard_map/mul | solution.py:272
  40.5 1.2 %copy.21 = bf16[128,8,2,256]{3,1,2,0:T(8,128)(2,1)} copy(bf16[128,8,2,256]{3,2,1,0:T(2,128)(2,1)S(1)} %bitcast.20) | data formatting | bytes 2097152
  41.9 1.8 %pad_maximum_fusion.2.query_w_ref = bf16[2048,256]{1,0:T(8,128)(2,1)S(1)} fusion(bf16[2048,64]{1,0:T(8,128)(2,1)} %slice.13, bf16[2048,192]{1,0:T(8,128)(2,1)} %copy.20), kind=kLoop, calls=%fused_computation.2 | loop fusion | flops 2097152 | bytes 2097152 | tf_op jit(solution)/shard_map/concatenate | solution.py:269
  43.7 0.8 %project_second.1 = (bf16[2,256,256]{2,1,0:T(8,128)(2,1)S(1)}, f32[256,128]{1,0:T(8,128)S(1)}) custom-call(bf16[256,2048]{1,0:T(8,128)(2,1)S(1)} %get-tuple-element.16.scaled_ref, f32[256,128]{1,0:T(8,128)S(1)} %copy-done.3, bf16[2048,256]{1,0:T(8,128)(2,1)S(1)} %pad_maximum_fusion.2.query_w_ref, bf16[2048,128]{1,0:T(8,128)(2,1)S(1)} %copy-done.1, ...), custom_call_target="tpu_custom_call" | custom-call | flops 402653184 | bytes 2097152 | tf_op jit(solution)/shard_map/project_second/pallas_call | solution.py:31
  45.0 4.4 %attend.1 = (bf16[128,256]{1,0:T(8,128)(2,1)S(1)}, bf16[128,256]{1,0:T(8,128)(2,1)S(1)}, f32[1,256]{1,0:T(1,128)}) custom-call(bf16[4,4,144,128]{3,2,1,0:T(8,128)(2,1)} %pad_maximum_fusion.3.even_ref, bf16[4,4,144,128]{3,2,1,0:T(8,128)(2,1)} %collective-permute-done.10.odd_ref, bf16[4,16,128]{2,1,0:T(8,128)(2,1)S(1)} %pad_maximum_fusion.6.halo_ref, ...), custom_call_target="tpu_custom_call" | custom-call | flops 1073741824 | bytes 4194304 | tf_op jit(solution)/shard_map/attend/pallas_call | solution.py:31
  49.9 0.9 %collective-permute-done.11.got_ref = bf16[128,256]{1,0:T(8,128)(2,1)S(1)} collective-permute-done((bf16[128,256]{1,0:T(8,128)(2,1)S(1)}, bf16[128,256]{1,0:T(8,128)(2,1)S(1)}, u32[]{:S(2)}, u32[]{:S(2)}) %collective-permute-start.11) | collective-permute-done | bytes 65568 | tf_op jit(solution)/shard_map/ppermute | solution.py:24
  51.2 1.2 %collective-permute-start.13 = (bf16[32,2048]{1,0:T(8,128)(2,1)S(1)}, bf16[32,2048]{1,0:T(8,128)(2,1)S(1)}, u32[]{:S(2)}, u32[]{:S(2)}) collective-permute-start(bf16[32,2048]{1,0:T(8,128)(2,1)S(1)} %get-tuple-element.24), channel_id=1, source_target_pairs={{0,2},{1,3},{2,0},{3,1},{4,6},{5,7},{6,4},{7,5},{8,10},{9,11},{10,... | collective-permute-start | bytes 393224 | tf_op jit(solution)/shard_map/ppermute | solution.py:24
  52.5 0.9 %collective-permute-start.14 = (bf16[32,2048]{1,0:T(8,128)(2,1)S(1)}, bf16[32,2048]{1,0:T(8,128)(2,1)S(1)}, u32[]{:S(2)}, u32[]{:S(2)}) collective-permute-start(bf16[32,2048]{1,0:T(8,128)(2,1)S(1)} %get-tuple-element.25), channel_id=1, source_target_pairs={{0,4},{1,5},{2,6},{3,7},{4,0},{5,1},{6,2},{7,3},{8,12},{9,13},{10,... | collective-permute-start | bytes 393224 | tf_op jit(solution)/shard_map/ppermute | solution.py:24
  53.3 1.4 %collective-permute-start.15 = (bf16[32,2048]{1,0:T(8,128)(2,1)S(1)}, bf16[32,2048]{1,0:T(8,128)(2,1)S(1)}, u32[]{:S(2)}, u32[]{:S(2)}) collective-permute-start(bf16[32,2048]{1,0:T(8,128)(2,1)S(1)} %get-tuple-element.26), channel_id=1, source_target_pairs={{0,6},{1,7},{2,4},{3,5},{4,2},{5,3},{6,0},{7,1},{8,14},{9,15},{10,... | collective-permute-start | bytes 393224 | tf_op jit(solution)/shard_map/ppermute | solution.py:24
  54.8 2.9 %collective-permute-done.13 = bf16[32,2048]{1,0:T(8,128)(2,1)S(1)} collective-permute-done((bf16[32,2048]{1,0:T(8,128)(2,1)S(1)}, bf16[32,2048]{1,0:T(8,128)(2,1)S(1)}, u32[]{:S(2)}, u32[]{:S(2)}) %collective-permute-start.13) | collective-permute-done | bytes 131104 | tf_op jit(solution)/shard_map/ppermute | solution.py:24
  57.7 1.5 %collective-permute-done.14 = bf16[32,2048]{1,0:T(8,128)(2,1)S(1)} collective-permute-done((bf16[32,2048]{1,0:T(8,128)(2,1)S(1)}, bf16[32,2048]{1,0:T(8,128)(2,1)S(1)}, u32[]{:S(2)}, u32[]{:S(2)}) %collective-permute-start.14) | collective-permute-done | bytes 131104 | tf_op jit(solution)/shard_map/ppermute | solution.py:24
  59.2 1.6 %collective-permute-done.15 = bf16[32,2048]{1,0:T(8,128)(2,1)S(1)} collective-permute-done((bf16[32,2048]{1,0:T(8,128)(2,1)S(1)}, bf16[32,2048]{1,0:T(8,128)(2,1)S(1)}, u32[]{:S(2)}, u32[]{:S(2)}) %collective-permute-start.15) | collective-permute-done | bytes 131104 | tf_op jit(solution)/shard_map/ppermute | solution.py:24
  60.8 0.7 %add_convert_fusion = bf16[32,2048]{1,0:T(8,128)(2,1)} fusion(bf16[32,2048]{1,0:T(8,128)(2,1)S(1)} %collective-permute-done.15, bf16[32,2048]{1,0:T(8,128)(2,1)S(1)} %collective-permute-done.14, f32[32,2048]{1,0:T(8,128)S(1)} %get-tuple-element.23, bf16[32,2048]{1,0:T(8,128)(2,1)S(1)} %collective-permute-done.13), kind=kLoop, calls=%fused_computation.6 | loop fusion | flops 458752 | bytes 786432 | tf_op jit(solution)/shard_map/convert_element_type | solution.py:335
  (69 shorter events, 4.6 us)
Async XLA Ops:
  0.6 12.1 %copy-start.9 = (bf16[2048,64]{0,1:T(8,128)(2,1)S(1)}, bf16[2048,64]{0,1:T(8,128)(2,1)}, u32[]{:S(2)}) copy-start(bf16[2048,64]{0,1:T(8,128)(2,1)} %param.16) | copy-start | bytes 786436
  0.6 12.4 %copy-start.10 = (bf16[2048,64]{0,1:T(8,128)(2,1)S(1)}, bf16[2048,64]{0,1:T(8,128)(2,1)}, u32[]{:S(2)}) copy-start(bf16[2048,64]{0,1:T(8,128)(2,1)} %param.17) | copy-start | bytes 786436
  0.6 7.2 %collective-permute-start = (bf16[256,256]{1,0:T(8,128)(2,1)}, bf16[256,256]{1,0:T(8,128)(2,1)S(1)}, u32[]{:S(2)}, u32[]{:S(2)}) collective-permute-start(bf16[256,256]{1,0:T(8,128)(2,1)} %param.13), channel_id=1, source_target_pairs={{0,2},{1,3},{2,0},{3,1},{4,6},{5,7},{6,4},{7,5},{8,10},{9,11},{10,... | collective-permute-start | bytes 393224 | tf_op jit(solution)/shard_map/ppermute | solution.py:24
  3.7 8.0 %collective-permute-start.1 = (bf16[256,256]{1,0:T(8,128)(2,1)}, bf16[256,256]{1,0:T(8,128)(2,1)S(1)}, u32[]{:S(2)}, u32[]{:S(2)}) collective-permute-start(bf16[256,256]{1,0:T(8,128)(2,1)} %param.13), channel_id=1, source_target_pairs={{0,4},{1,5},{2,6},{3,7},{4,0},{5,1},{6,2},{7,3},{8,12},{9,13},{10,... | collective-permute-start | bytes 393224 | tf_op jit(solution)/shard_map/ppermute | solution.py:24
  5.2 6.5 %collective-permute-start.2 = (bf16[256,256]{1,0:T(8,128)(2,1)}, bf16[256,256]{1,0:T(8,128)(2,1)S(1)}, u32[]{:S(2)}, u32[]{:S(2)}) collective-permute-start(bf16[256,256]{1,0:T(8,128)(2,1)} %param.13), channel_id=1, source_target_pairs={{0,6},{1,7},{2,4},{3,5},{4,2},{5,3},{6,0},{7,1},{8,14},{9,15},{10,... | collective-permute-start | bytes 393224 | tf_op jit(solution)/shard_map/ppermute | solution.py:24
  12.7 1.3 %copy-start.8 = (bf16[2048,128]{1,0:T(8,128)(2,1)S(1)}, bf16[2048,128]{1,0:T(8,128)(2,1)}, u32[]{:S(2)}) copy-start(bf16[2048,128]{1,0:T(8,128)(2,1)} %param.22) | copy-start | bytes 1572868
  12.7 3.1 %collective-permute-start.3 = (bf16[4,256,256]{2,1,0:T(8,128)(2,1)S(1)}, bf16[4,256,256]{2,1,0:T(8,128)(2,1)S(1)}, u32[]{:S(2)}, u32[]{:S(2)}) collective-permute-start(bf16[4,256,256]{2,1,0:T(8,128)(2,1)S(1)} %pad_maximum_fusion.4.even_ref), channel_id=1, source_target_pairs={{0,1},{1,0},{2,3},{3,2},{4,5},{5,4},{6,7},{7,6},{8,9},{9,8},{10,11... | collective-permute-start | bytes 1572872 | tf_op jit(solution)/shard_map/ppermute | solution.py:24
  15.8 6.2 %copy-start.6 = (bf16[128,2048]{1,0:T(8,128)(2,1)S(1)}, bf16[128,2048]{1,0:T(8,128)(2,1)}, u32[]{:S(2)}) copy-start(bf16[128,2048]{1,0:T(8,128)(2,1)} %param.24) | copy-start | bytes 1572868
  17.6 14.2 %copy-start.7 = (bf16[128,2048]{1,0:T(8,128)(2,1)S(1)}, bf16[128,2048]{1,0:T(8,128)(2,1)}, u32[]{:S(2)}) copy-start(bf16[128,2048]{1,0:T(8,128)(2,1)} %param.25) | copy-start | bytes 1572868
  17.6 4.4 %collective-permute-start.4 = (bf16[160,128]{1,0:T(8,128)(2,1)S(1)}, bf16[160,128]{1,0:T(8,128)(2,1)S(1)}, u32[]{:S(2)}, u32[]{:S(2)}) collective-permute-start(bf16[160,128]{1,0:T(8,128)(2,1)S(1)} %get-tuple-element.15), channel_id=1, source_target_pairs={{0,8},{8,0},{16,24},{24,16},{1,9},{9,1},{17,25},{25,17},{2,10},{10... | collective-permute-start | bytes 122888 | tf_op jit(solution)/shard_map/ppermute | solution.py:24
  19.2 5.7 %collective-permute-start.5 = (bf16[160,128]{1,0:T(8,128)(2,1)S(1)}, bf16[160,128]{1,0:T(8,128)(2,1)S(1)}, u32[]{:S(2)}, u32[]{:S(2)}) collective-permute-start(bf16[160,128]{1,0:T(8,128)(2,1)S(1)} %get-tuple-element.15), channel_id=1, source_target_pairs={{0,16},{8,24},{16,0},{24,8},{1,17},{9,25},{17,1},{25,9},{2,18},{10... | collective-permute-start | bytes 122888 | tf_op jit(solution)/shard_map/ppermute | solution.py:24
  21.7 5.8 %collective-permute-start.6 = (bf16[160,128]{1,0:T(8,128)(2,1)S(1)}, bf16[160,128]{1,0:T(8,128)(2,1)S(1)}, u32[]{:S(2)}, u32[]{:S(2)}) collective-permute-start(bf16[160,128]{1,0:T(8,128)(2,1)S(1)} %get-tuple-element.15), channel_id=1, source_target_pairs={{0,24},{8,16},{16,8},{24,0},{1,25},{9,17},{17,9},{25,1},{2,26},{10... | collective-permute-start | bytes 122888 | tf_op jit(solution)/shard_map/ppermute | solution.py:24
  22.0 9.8 %copy-start.12 = (bf16[160,128]{1,0:T(8,128)(2,1)}, bf16[160,128]{1,0:T(8,128)(2,1)S(1)}, u32[]{:S(2)}) copy-start(bf16[160,128]{1,0:T(8,128)(2,1)S(1)} %collective-permute-done.4) | copy-start | bytes 122884
  24.9 7.0 %copy-start.14 = (bf16[160,128]{1,0:T(8,128)(2,1)}, bf16[160,128]{1,0:T(8,128)(2,1)S(1)}, u32[]{:S(2)}) copy-start(bf16[160,128]{1,0:T(8,128)(2,1)S(1)} %collective-permute-done.5) | copy-start | bytes 122884
  27.5 4.3 %copy-start.16 = (bf16[160,128]{1,0:T(8,128)(2,1)}, bf16[160,128]{1,0:T(8,128)(2,1)S(1)}, u32[]{:S(2)}) copy-start(bf16[160,128]{1,0:T(8,128)(2,1)S(1)} %collective-permute-done.6) | copy-start | bytes 122884
  28.3 7.8 %collective-permute-start.8 = (bf16[4,144,128]{2,1,0:T(8,128)(2,1)}, bf16[4,144,128]{2,1,0:T(8,128)(2,1)}, u32[]{:S(2)}, u32[]{:S(2)}) collective-permute-start(bf16[4,144,128]{2,1,0:T(8,128)(2,1)} %get-tuple-element.29), channel_id=1, source_target_pairs={{0,4},{1,5},{2,6},{3,7},{4,0},{5,1},{6,2},{7,3},{8,12},{9,13},{10,... | collective-permute-start | bytes 442376 | tf_op jit(solution)/shard_map/ppermute | solution.py:24
  29.8 7.0 %collective-permute-start.9 = (bf16[4,144,128]{2,1,0:T(8,128)(2,1)}, bf16[4,144,128]{2,1,0:T(8,128)(2,1)}, u32[]{:S(2)}, u32[]{:S(2)}) collective-permute-start(bf16[4,144,128]{2,1,0:T(8,128)(2,1)} %get-tuple-element.29), channel_id=1, source_target_pairs={{0,6},{1,7},{2,4},{3,5},{4,2},{5,3},{6,0},{7,1},{8,14},{9,15},{10,... | collective-permute-start | bytes 442376 | tf_op jit(solution)/shard_map/ppermute | solution.py:24
  31.0 6.5 %collective-permute-start.7 = (bf16[4,144,128]{2,1,0:T(8,128)(2,1)}, bf16[4,144,128]{2,1,0:T(8,128)(2,1)}, u32[]{:S(2)}, u32[]{:S(2)}) collective-permute-start(bf16[4,144,128]{2,1,0:T(8,128)(2,1)} %get-tuple-element.29), channel_id=1, source_target_pairs={{0,2},{1,3},{2,0},{3,1},{4,6},{5,7},{6,4},{7,5},{8,10},{9,11},{10,... | collective-permute-start | bytes 442376 | tf_op jit(solution)/shard_map/ppermute | solution.py:24
  31.9 18.0 %collective-permute-start.12 = (bf16[256,2048]{1,0:T(8,128)(2,1)S(1)}, bf16[256,2048]{1,0:T(8,128)(2,1)S(1)}, u32[]{:S(2)}, u32[]{:S(2)}) collective-permute-start(bf16[256,2048]{1,0:T(8,128)(2,1)S(1)} %constant_dynamic-update-slice_fusion.own_w_ref), channel_id=1, source_target_pairs={{0,1},{1,0},{2,3},{3,2},{4,5},{5,4},{6,7},{7,6},{8,9},{9,8},{10,11... | collective-permute-start | bytes 3145736 | tf_op jit(solution)/shard_map/ppermute | solution.py:24
  34.2 3.4 %copy-start.5 = (bf16[1,4,144,128]{3,2,1,0:T(8,128)(2,1)S(1)}, bf16[1,4,144,128]{3,2,1,0:T(8,128)(2,1)}, u32[]{:S(2)}) copy-start(bf16[1,4,144,128]{3,2,1,0:T(8,128)(2,1)} %get-tuple-element.28) | copy-start | bytes 442372
  34.2 5.3 %copy-start.11 = (bf16[512,256]{1,0:T(8,128)(2,1)S(1)}, bf16[512,256]{1,0:T(8,128)(2,1)}, u32[]{:S(2)}) copy-start(bf16[512,256]{1,0:T(8,128)(2,1)} %param.19) | copy-start | bytes 786436
  39.5 5.1 %collective-permute-start.10 = (bf16[4,4,144,128]{3,2,1,0:T(8,128)(2,1)}, bf16[4,4,144,128]{3,2,1,0:T(8,128)(2,1)}, u32[]{:S(2)}, u32[]{:S(2)}) collective-permute-start(bf16[4,4,144,128]{3,2,1,0:T(8,128)(2,1)} %pad_maximum_fusion.3.even_ref), channel_id=1, source_target_pairs={{0,1},{1,0},{2,3},{3,2},{4,5},{5,4},{6,7},{7,6},{8,9},{9,8},{10,11... | collective-permute-start | bytes 1769480 | tf_op jit(solution)/shard_map/ppermute | solution.py:24
  40.5 1.2 %copy-start.19 = (f32[512]{0:T(512)S(1)}, f32[512]{0:T(512)}, u32[]{:S(2)}) copy-start(f32[512]{0:T(512)} %param.18) | copy-start | bytes 6148
  41.9 1.8 %copy-start.1 = (bf16[2048,128]{1,0:T(8,128)(2,1)S(1)}, bf16[2048,128]{1,0:T(8,128)(2,1)}, u32[]{:S(2)}) copy-start(bf16[2048,128]{1,0:T(8,128)(2,1)} %gate_w_ref.1) | copy-start | bytes 1572868
  41.9 1.8 %copy-start.3 = (f32[256,128]{1,0:T(8,128)S(1)}, f32[256,128]{1,0:T(8,128)}, u32[]{:S(2)}) copy-start(f32[256,128]{1,0:T(8,128)} %copy-done.2) | copy-start | bytes 393220
  43.7 0.8 %copy-start.13 = (bf16[160,128]{1,0:T(8,128)(2,1)S(1)}, bf16[160,128]{1,0:T(8,128)(2,1)}, u32[]{:S(2)}) copy-start(bf16[160,128]{1,0:T(8,128)(2,1)} %copy-done.12) | copy-start | bytes 122884
  43.7 1.3 %copy-start = (bf16[128,8,2,256]{3,1,2,0:T(8,128)(2,1)S(1)}, bf16[128,8,2,256]{3,1,2,0:T(8,128)(2,1)}, u32[]{:S(2)}) copy-start(bf16[128,8,2,256]{3,1,2,0:T(8,128)(2,1)} %copy.21) | copy-start | bytes 3145732
  43.7 1.3 %copy-start.4 = (bf16[3,128]{1,0:T(4,128)(2,1)S(1)}, bf16[3,128]{1,0:T(4,128)(2,1)}, u32[]{:S(2)}) copy-start(bf16[3,128]{1,0:T(4,128)(2,1)} %taps_ref.1) | copy-start | bytes 2308
  49.4 1.4 %collective-permute-start.11 = (bf16[128,256]{1,0:T(8,128)(2,1)S(1)}, bf16[128,256]{1,0:T(8,128)(2,1)S(1)}, u32[]{:S(2)}, u32[]{:S(2)}) collective-permute-start(bf16[128,256]{1,0:T(8,128)(2,1)S(1)} %get-tuple-element.22), channel_id=1, source_target_pairs={{0,1},{1,0},{2,3},{3,2},{4,5},{5,4},{6,7},{7,6},{8,9},{9,8},{10,11... | collective-permute-start | bytes 196616 | tf_op jit(solution)/shard_map/ppermute | solution.py:24
  51.2 6.4 %collective-permute-start.13 = (bf16[32,2048]{1,0:T(8,128)(2,1)S(1)}, bf16[32,2048]{1,0:T(8,128)(2,1)S(1)}, u32[]{:S(2)}, u32[]{:S(2)}) collective-permute-start(bf16[32,2048]{1,0:T(8,128)(2,1)S(1)} %get-tuple-element.24), channel_id=1, source_target_pairs={{0,2},{1,3},{2,0},{3,1},{4,6},{5,7},{6,4},{7,5},{8,10},{9,11},{10,... | collective-permute-start | bytes 393224 | tf_op jit(solution)/shard_map/ppermute | solution.py:24
  52.5 6.7 %collective-permute-start.14 = (bf16[32,2048]{1,0:T(8,128)(2,1)S(1)}, bf16[32,2048]{1,0:T(8,128)(2,1)S(1)}, u32[]{:S(2)}, u32[]{:S(2)}) collective-permute-start(bf16[32,2048]{1,0:T(8,128)(2,1)S(1)} %get-tuple-element.25), channel_id=1, source_target_pairs={{0,4},{1,5},{2,6},{3,7},{4,0},{5,1},{6,2},{7,3},{8,12},{9,13},{10,... | collective-permute-start | bytes 393224 | tf_op jit(solution)/shard_map/ppermute | solution.py:24
  53.3 7.4 %collective-permute-start.15 = (bf16[32,2048]{1,0:T(8,128)(2,1)S(1)}, bf16[32,2048]{1,0:T(8,128)(2,1)S(1)}, u32[]{:S(2)}, u32[]{:S(2)}) collective-permute-start(bf16[32,2048]{1,0:T(8,128)(2,1)S(1)} %get-tuple-element.26), channel_id=1, source_target_pairs={{0,6},{1,7},{2,4},{3,5},{4,2},{5,3},{6,0},{7,1},{8,14},{9,15},{10,... | collective-permute-start | bytes 393224 | tf_op jit(solution)/shard_map/ppermute | solution.py:24
  (4 other events, 3.1 us)

commit v2 on v1

v2 whole, which is shorter than its diff:
```python
import functools
import math

import jax
import jax.numpy as jnp
from jax import lax
from jax.experimental import pallas as pl
from jax.experimental.pallas import tpu as pltpu
from jax.sharding import PartitionSpec as P

NOPE = 128
ROPE = 64
VDIM = 128
GRID_W = 64
EPSILON = 1e-06
ROPE_BASE = 10000.0
LANES = 128
HALO = 8
F32 = jnp.float32
BF16 = jnp.bfloat16


def swap(array, axis, mask):
    peers = lax.axis_size(axis)
    return lax.ppermute(array, axis, [(i, i ^ mask) for i in range(peers)])


def kernel_call(body, outs, limit, scratch=(), flops=0, nbytes=0, name=None):
    whole = pl.BlockSpec(memory_space=pltpu.VMEM)

    def call(*operands):
        return pl.pallas_call(
            body,
            out_shape=[jax.ShapeDtypeStruct(shape, dtype) for shape, dtype in outs],
            in_specs=[whole] * len(operands),
            out_specs=[whole] * len(outs),
            scratch_shapes=list(scratch),
            compiler_params=pltpu.CompilerParams(vmem_limit_bytes=limit),
            cost_estimate=pl.CostEstimate(flops=flops, bytes_accessed=nbytes, transcendentals=0),
            name=name,
        )(*operands)

    return call


def rotate(values, cosines, sines):
    quarter = ROPE // 4
    lane = lax.broadcasted_iota(jnp.int32, values.shape, 1)
    first = (lane // quarter) % 2 == 0
    ahead = pltpu.roll(values, LANES - quarter, 1)
    behind = pltpu.roll(values, quarter, 1)
    return values * cosines + jnp.where(first, ahead, behind) * sines


def low_lanes(shape):
    return lax.broadcasted_iota(jnp.int32, shape, 1) < ROPE


def prepare(
    latent_ref, rope_ref, query_ref, pre_ref, value_ref, expand_ref, gain_ref, attend_ref, conv_ref,
    key_w_ref, query_w_ref, mix_w_ref, expand_k_ref, expand_v_ref, lat_gain_ref, own_w_ref, cos_ref, sin_ref,
):
    own_w_ref[:VDIM, :] = attend_ref[...]
    own_w_ref[VDIM:, :] = conv_ref[...]
    for i in range(2):
        key_w_ref[i * ROPE : (i + 1) * ROPE, :] = latent_ref[...]
        key_w_ref[(i + 2) * ROPE : (i + 3) * ROPE, :] = rope_ref[...]
    query_w_ref[: NOPE + ROPE, :] = query_ref[...]
    query_w_ref[NOPE + ROPE :, :] = query_ref[NOPE:, :]
    mix_w_ref[:, :LANES] = pre_ref[...]
    mix_w_ref[:, LANES:] = value_ref[...]
    ranks = lat_gain_ref.shape[0]
    low = low_lanes((1, LANES))
    zeros = jnp.zeros((ROPE, LANES), BF16)
    for k in range(ranks):
        part = expand_ref[k * ROPE : (k + 1) * ROPE, :]
        upper = slice(k * LANES, k * LANES + ROPE)
        lower = slice(k * LANES + ROPE, (k + 1) * LANES)
        for ref, piece in ((expand_k_ref, part[:, :NOPE]), (expand_v_ref, part[:, NOPE:])):
            ref[upper, :LANES] = piece
            ref[upper, LANES:] = zeros
            ref[lower, :LANES] = zeros
            ref[lower, LANES:] = piece
        pair = gain_ref[:, (k // 2) * LANES : (k // 2 + 1) * LANES]
        turned = pltpu.roll(pair, ROPE, 1)
        chosen = (pair, turned) if k % 2 == 0 else (turned, pair)
        lat_gain_ref[k : k + 1, :] = jnp.where(low, *chosen)
    quarter = ROPE // 4
    groups = cos_ref.shape[0] // GRID_W
    first_row = lax.axis_index("sp") * groups

    def angles(rows, start):
        lane = lax.broadcasted_iota(jnp.int32, (rows, LANES), 1) % ROPE
        place = (lax.broadcasted_iota(jnp.int32, (rows, LANES), 0) + start).astype(F32)
        inverse = jnp.exp((lane % quarter).astype(F32) * (-math.log(ROPE_BASE) / quarter))
        angle = place * inverse
        sign = jnp.where((lane // quarter) % 2 == 0, -1.0, 1.0)
        return lane < 2 * quarter, jnp.cos(angle), jnp.sin(angle) * sign

    _, row_cos, row_sin = angles(groups, first_row)
    by_row, col_cos, col_sin = angles(GRID_W, 0)
    for g in range(groups):
        rows = slice(g * GRID_W, (g + 1) * GRID_W)
        cos_ref[rows, :] = jnp.where(by_row, row_cos[g : g + 1], col_cos)
        sin_ref[rows, :] = jnp.where(by_row, row_sin[g : g + 1], col_sin)


def dot_nt(left, right):
    return lax.dot_general(left, right, (((1,), (1,)), ((), ())), preferred_element_type=F32)


def project_first(pairs, *refs):
    pieces, refs = refs[: 2 * pairs], refs[2 * pairs :]
    gain_ref, key_w_ref, mix_w_ref, cos_ref, sin_ref = refs[:5]
    scaled_ref, inv_ref, message_ref, mix_ref, key_ref = refs[5:]
    rank = lax.axis_index("tp")
    tokens, width = pieces[0].shape
    half = tokens // 2
    total = jnp.zeros((tokens, LANES), F32)
    for i, ref in enumerate(pieces):
        owner = rank ^ (2 * (i % pairs) + i // pairs)
        piece = ref[...].astype(F32)
        squares = piece * piece
        for j in range(width // LANES):
            total = total + squares[:, j * LANES : (j + 1) * LANES]
        columns = pl.ds(pl.multiple_of(owner * width, width), width)
        scaled_ref[:, columns] = (piece * gain_ref[:, columns]).astype(BF16)
    features = 2 * pairs * width
    inv = lax.rsqrt(jnp.sum(total, axis=1, keepdims=True) / features + EPSILON)
    inv_ref[...] = jnp.broadcast_to(inv, inv_ref.shape)
    scaled = scaled_ref[...]
    keys = dot_nt(scaled, key_w_ref[...]) * inv
    mixes = jnp.dot(scaled, mix_w_ref[...], preferred_element_type=F32) * inv
    mix = (mixes[:, :LANES] * mixes[:, LANES:]).astype(BF16)
    mix_ref[...] = mix
    latent = keys[:, :LANES]
    low = low_lanes((half, LANES))
    message_ref[:half, :] = jnp.where(low, latent[:half], latent[half:]).astype(BF16)
    key_ref[...] = keys[:, LANES:]
    share = half // (2 * pairs)
    start = pl.multiple_of(rank * share, share)
    turned = []
    for base in (0, half):
        rows = pl.ds(start + base, share)
        turned.append(rotate(key_ref[rows, :], cos_ref[rows, :], sin_ref[rows, :]))
    low = low_lanes((share, LANES))
    message_ref[half : half + share, :] = jnp.where(low, turned[0], turned[1]).astype(BF16)
    row = lax.broadcasted_iota(jnp.int32, (HALO, LANES), 0)
    first = jnp.broadcast_to(mix[:1].astype(F32), (HALO, LANES))
    last = jnp.broadcast_to(mix[tokens - 1 :].astype(F32), (HALO, LANES))
    message_ref[half + share :, :] = jnp.where(row == 0, first, last).astype(BF16)


def project_second(
    scaled_ref, inv_ref, query_w_ref, gate_w_ref, cos_ref, sin_ref, query_ref, gate_ref
):
    scaled = scaled_ref[...]
    inv = inv_ref[...]
    scale = (NOPE + ROPE) ** (-0.5)
    query = dot_nt(scaled, query_w_ref[...])
    gate_ref[...] = jnp.dot(scaled, gate_w_ref[...], preferred_element_type=F32) * inv
    nope = (query[:, :NOPE] * inv * scale).astype(BF16)
    rope = rotate(query[:, NOPE:] * inv, cos_ref[...], sin_ref[...]) * scale
    low = low_lanes(rope.shape)
    query_ref[0, :, :NOPE] = nope
    query_ref[1, :, :NOPE] = nope
    query_ref[0, :, NOPE:] = jnp.where(low, rope, 0.0).astype(BF16)
    query_ref[1, :, NOPE:] = jnp.where(low, 0.0, rope).astype(BF16)


def attend(pairs, chunk, natural, *refs):
    pieces, refs = refs[: 2 * pairs], refs[2 * pairs :]
    gain_ref, expand_k_ref, expand_v_ref, query_ref, gate_ref, mix_ref, taps_ref = refs[:7]
    keep_ref, send_ref, log_ref, latent_ref, rope_ref, both_ref = refs[7:]
    rank = lax.axis_index("tp")
    place = lax.axis_index("sp")
    blocks = pieces[0].shape[0]
    ranks = 2 * pairs
    tokens = query_ref.shape[1]
    half = tokens // 2
    share = half // ranks
    entries = ranks * ROPE
    low = low_lanes((half, LANES))
    owned = [(rank ^ (2 * (i % pairs) + i // pairs), ref) for i, ref in enumerate(pieces)]

    def one_chunk(first, state):
        for slot in range(chunk):
            block = first + slot
            base = slot * half
            total = jnp.zeros((half, LANES), F32)
            for owner, ref in owned:
                piece = ref[block, :half, :].astype(F32)
                total = total + piece * piece
                start = pl.multiple_of(base + owner * share, share)
                rope_ref[pl.ds(start, share), :] = ref[block, half : half + share, :]
            sum_low = jnp.sum(jnp.where(low, total, 0.0), axis=1, keepdims=True)
            sum_high = jnp.sum(jnp.where(low, 0.0, total), axis=1, keepdims=True)
            inv = lax.rsqrt(jnp.where(low, sum_low, sum_high) / entries + EPSILON)
            for owner, ref in owned:
                piece = ref[block, :half, :].astype(F32)
                start = pl.multiple_of(owner * LANES, LANES)
                scaled = piece * inv * gain_ref[pl.ds(owner, 1), :]
                latent_ref[base : base + half, pl.ds(start, LANES)] = scaled.astype(BF16)
        latent = latent_ref[...]
        keys = jnp.dot(latent, expand_k_ref[...], preferred_element_type=F32).astype(BF16)
        values = lax.dot_general(
            expand_v_ref[...], latent, (((0,), (1,)), ((), ())), preferred_element_type=F32
        ).astype(BF16)
        rope = rope_ref[...]
        scores = [
            dot_nt(jnp.concatenate([keys[:, i * NOPE : (i + 1) * NOPE], rope], axis=1), query_ref[i])
            for i in range(2)
        ]
        peak = jnp.max(jnp.maximum(*scores), axis=0, keepdims=True)
        if state is not None:
            peak = jnp.maximum(peak, state[0])
        weights = [jnp.exp(piece - peak) for piece in scores]
        total = jnp.sum(weights[0] + weights[1], axis=0, keepdims=True)
        out = sum(
            jnp.dot(values[i * VDIM : (i + 1) * VDIM], weights[i].astype(BF16), preferred_element_type=F32)
            for i in range(2)
        )
        if state is not None:
            rescale = jnp.exp(state[0] - peak)
            total = total + state[1] * rescale
            out = out + state[2] * rescale
        return peak, total, out

    if blocks == chunk:
        peak, total, out = one_chunk(0, None)
    else:
        start = (
            jnp.full((1, tokens), -jnp.inf, F32),
            jnp.zeros((1, tokens), F32),
            jnp.zeros((VDIM, tokens), F32),
        )
        peak, total, out = lax.fori_loop(0, blocks // chunk, lambda i, state: one_chunk(i * chunk, state), start)
    both_ref[:, :VDIM] = jnp.transpose(out / total)
    log_ref[...] = peak + jnp.log(total)

    mix = mix_ref[...].astype(F32)
    before_at = jnp.maximum(place - 1, 0)
    after_at = jnp.minimum(place + 1, blocks - 1)
    if not natural:
        before_at, after_at = before_at ^ place, after_at ^ place
    edge = half + share
    before = jnp.where(place > 0, pieces[0][before_at, edge:, :].astype(F32)[1:2, :], 0.0)
    after = jnp.where(place < blocks - 1, pieces[0][after_at, edge:, :].astype(F32)[0:1, :], 0.0)
    row = lax.broadcasted_iota(jnp.int32, mix.shape, 0)
    earlier = jnp.where(row == 0, before, pltpu.roll(mix, 1, 0))
    later = jnp.where(row == tokens - 1, after, pltpu.roll(mix, tokens - 1, 0))
    taps = taps_ref[...].astype(F32)
    convolved = taps[0:1] * earlier + taps[1:2] * mix + taps[2:3] * later
    both_ref[:, VDIM:] = gate_ref[...] * convolved

    chip, core = rank // 2, rank % 2
    rows = tokens // ranks
    for i in range(pairs):
        base = 2 * (chip ^ i)
        mine = pl.multiple_of((base + core) * rows, rows)
        other = pl.multiple_of((base + 1 - core) * rows, rows)
        keep_ref[i * rows : (i + 1) * rows, :] = both_ref[pl.ds(mine, rows), :].astype(BF16)
        send_ref[i * rows : (i + 1) * rows, :] = both_ref[pl.ds(other, rows), :].astype(BF16)


def output(keep_ref, got_ref, own_w_ref, other_w_ref, first_ref, *rest_refs):
    out = jnp.dot(keep_ref[...], own_w_ref[...], preferred_element_type=F32)
    out = out + jnp.dot(got_ref[...], other_w_ref[...], preferred_element_type=F32)
    rows = first_ref.shape[0]
    first_ref[...] = out[:rows]
    for i, ref in enumerate(rest_refs):
        ref[...] = out[(i + 1) * rows : (i + 2) * rows].astype(BF16)


def body(
    activations,
    norm_gain,
    query_weight,
    latent_weight,
    rope_key_weight,
    latent_gain,
    expand_weight,
    gate_weight,
    pre_weight,
    value_weight,
    conv_kernel,
    output_attend,
    output_conv,
):
    ranks = lax.axis_size("tp")
    places = lax.axis_size("sp")
    pairs = ranks // 2
    tokens, width = activations.shape
    features = ranks * width
    half = tokens // 2
    share = half // ranks
    rows = tokens // ranks
    channels = gate_weight.shape[1]

    far = [swap(activations, "tp", 2 * i) for i in reversed(range(1, pairs))][::-1]
    even = [activations] + far
    odd = [swap(piece, "tp", 1) for piece in even]

    key_w, query_w, mix_w, expand_k, expand_v, lat_gain, own_w, cosines, sines = kernel_call(
        prepare,
        [
            ((4 * ROPE, features), BF16),
            ((NOPE + 2 * ROPE, features), BF16),
            ((features, 2 * LANES), BF16),
            ((ranks * LANES, 2 * NOPE), BF16),
            ((ranks * LANES, 2 * VDIM), BF16),
            ((ranks, LANES), F32),
            ((VDIM + channels, features), BF16),
            ((tokens, LANES), F32),
            ((tokens, LANES), F32),
        ],
        16 << 20,
        flops=1 << 28,
        nbytes=1 << 23,
        name="prepare",
    )(
        latent_weight.T, rope_key_weight.T, query_weight.T, pre_weight, value_weight, expand_weight,
        latent_gain.reshape(1, -1), output_attend, output_conv,
    )
    other_w = swap(own_w, "tp", 1)

    scaled, inv, message, mix = kernel_call(
        functools.partial(project_first, pairs),
        [
            ((tokens, features), BF16),
            ((tokens, LANES), F32),
            ((half + share + HALO, LANES), BF16),
            ((tokens, channels), BF16),
        ],
        12 << 20,
        scratch=[pltpu.VMEM((tokens, LANES), F32)],
        flops=2 * tokens * features * 4 * LANES,
        nbytes=4 * tokens * features,
        name="project_first",
    )(*even, *odd, norm_gain.reshape(1, -1), key_w, mix_w, cosines, sines)

    small = places <= 8 and places & (places - 1) == 0
    if small:
        around = [swap(message, "sp", i) for i in reversed(range(1, places))][::-1]
        around = jnp.stack([message] + around)
    else:
        around = lax.all_gather(message, "sp", axis=0)
    query, gate = kernel_call(
        project_second,
        [((2, tokens, NOPE + LANES), BF16), ((tokens, channels), F32)],
        12 << 20,
        flops=2 * tokens * features * 3 * LANES,
        nbytes=4 * tokens * features,
        name="project_second",
    )(scaled, inv, query_w, gate_weight, cosines, sines)
    chip_far = [swap(around, "tp", 2 * i) for i in reversed(range(1, pairs))][::-1]
    chip_even = [around] + chip_far
    chip_odd = [swap(piece, "tp", 1) for piece in chip_even]

    chunk = places if small else 4
    keep, send, logs = kernel_call(
        functools.partial(attend, pairs, chunk, not small),
        [((half, VDIM + channels), BF16), ((half, VDIM + channels), BF16), ((1, tokens), F32)],
        (16 << 20) if small else (60 << 20),
        scratch=[
            pltpu.VMEM((chunk * half, ranks * LANES), BF16),
            pltpu.VMEM((chunk * half, LANES), BF16),
            pltpu.VMEM((tokens, VDIM + channels), F32),
        ],
        flops=1 << 30,
        nbytes=1 << 22,
        name="attend",
    )(*chip_even, *chip_odd, lat_gain, expand_k, expand_v, query, gate, mix, conv_kernel)

    got = swap(send, "tp", 1)
    outs = kernel_call(
        output,
        [((rows, features), F32)] + [((rows, features), BF16)] * (pairs - 1),
        12 << 20,
        flops=1 << 28,
        nbytes=1 << 22,
        name="output",
    )(keep, got, own_w, other_w)
    arrived = [swap(outs[i], "tp", 2 * i) for i in reversed(range(1, pairs))]
    total = outs[0]
    for piece in arrived:
        total = total + piece.astype(F32)
    return total.astype(BF16), logs


def solution(mesh):
    return jax.shard_map(
        body,
        mesh=mesh,
        in_specs=(
            P("sp", "tp"),
            P(),
            P(None, "tp"),
            P(None, "tp"),
            P(),
            P(),
            P(None, "tp"),
            P(None, "tp"),
            P(None, "tp"),
            P(None, "tp"),
            P(None, "tp"),
            P("tp", None),
            P("tp", None),
        ),
        out_specs=(P(("sp", "tp"), None), P("tp", "sp")),
        check_vma=False,
    )
```

time: 61.8 us -> 59.3 us (0.960)
  other arithmetic: 8.81 us -> 0.74 us
  waiting for transfers between devices: 20.2 us -> 25.1 us
  local copies, waits for them, and re-layouts: 8.06 us -> 9.51 us
  Pallas kernels: 6.75 us -> 5.47 us
    ppermute x16 -> x22, waiting for transfers between devices: 20.2 us -> 25.1 us  [swap(): return lax.ppermute(array, axis, [(i, i ^ mask) for i in range(peers)])]
    unnamed x45 -> x26, local copies, waits for them, and re-layouts: 5.19 us -> 9.51 us
    concatenate x2 -> x0, other arithmetic: 3.61 us -> none  [the longest x1 1.83 us: body(): jnp.concatenate([latent_weight, latent_weight, rope_key_weight, rope_key_...]
    another operation x3 -> x1, other arithmetic: 2.95 us -> 0.02 us  [body(): around = jnp.stack([message] + around)]
    slice x1 -> x0, local copies, waits for them, and re-layouts: 1.92 us -> none  [body(): query_w = jnp.concatenate([query_weight, query_weight[:, NOPE:]], axis=1)]
    mul x2 -> x0, other arithmetic: 1.49 us -> none  [the longest x1 0.95 us: body(): expand_w = (parts * eye).reshape(ranks * LANES, 2 * (NOPE + VDIM))]
    pallas_call x4 -> x5, Pallas kernels: 6.75 us -> 5.47 us  [call(): pl.pallas_call(body, out_shape=[jax.ShapeDtypeStruct(shape, dtype) for sh...]
    another operation x4 -> x0, local copies, waits for them, and re-layouts: 0.92 us -> none  [the longest x1 0.76 us: body(): jnp.stack([parts] + [swap(parts, 'tp', 2 * i) for i in range(1, pairs)])]
  transfers between devices with their start and end apart: 16 -> 22, of which waited for: 10 -> 15; matrix products, arithmetic and copies ran while one was open for 22% -> 0% of each run, Pallas kernels for 8% -> 7%
where the time goes in v2:
time: 59.3 us; the launch traced here: 58.8 us
  waiting for transfers between devices  25.1 us (42%)
  starting transfers between devices  17.3 us (29%)
  local copies, waits for them, and re-layouts  9.51 us (16%)
  Pallas kernels  5.47 us (9%)
  other arithmetic  0.74 us (1%)
  between operations  0.72 us (1%)
    ppermute x22, waiting for transfers between devices, swap(): return lax.ppermute(array, axis, [(i, i ^ mask) for i in range(peers)])  25.1 us
    ppermute x22, starting transfers between devices, swap(): return lax.ppermute(array, axis, [(i, i ^ mask) for i in range(peers)])  17.3 us
    unnamed x26, local copies, waits for them, and re-layouts  9.51 us
    pallas_call x5, Pallas kernels, call(): pl.pallas_call(body, out_shape=[jax.ShapeDtypeStruct(shape, dtype) for sh...  5.47 us
  transfers between devices with their start and end apart: 22, of which 15 were waited for; matrix products, arithmetic and copies ran while one was open for 0% of the time, Pallas kernels for 7%

profile of v2, /device:TPU:0, one launch (start us, length us, event | category | flops | bytes accessed | tf_op | source)
XLA Modules:
  0.0 58.8 jit_solution(290021046148349965)
XLA Ops:
  0.6 0.7 %copy-done.11 = f32[512]{0:T(512)S(1)} copy-done((f32[512]{0:T(512)S(1)}, f32[512]{0:T(512)}, u32[]{:S(2)}) %copy-start.11) | copy-done | bytes 2072
  1.3 1.1 %copy-done = bf16[2048,192]{0,1:T(8,128)(2,1)S(1)} copy-done((bf16[2048,192]{0,1:T(8,128)(2,1)S(1)}, bf16[2048,192]{0,1:T(8,128)(2,1)}, u32[]{:S(2)}) %copy-start) | copy-done | bytes 786456
  2.5 1.0 %copy-done.1 = bf16[2048,128]{1,0:T(8,128)(2,1)S(1)} copy-done((bf16[2048,128]{1,0:T(8,128)(2,1)S(1)}, bf16[2048,128]{1,0:T(8,128)(2,1)}, u32[]{:S(2)}) %copy-start.1) | copy-done | bytes 524312
  3.5 1.0 %copy-done.2 = bf16[2048,128]{1,0:T(8,128)(2,1)S(1)} copy-done((bf16[2048,128]{1,0:T(8,128)(2,1)S(1)}, bf16[2048,128]{1,0:T(8,128)(2,1)}, u32[]{:S(2)}) %copy-start.2) | copy-done | bytes 524312
  4.5 1.0 %copy-done.3 = bf16[128,2048]{1,0:T(8,128)(2,1)S(1)} copy-done((bf16[128,2048]{1,0:T(8,128)(2,1)S(1)}, bf16[128,2048]{1,0:T(8,128)(2,1)}, u32[]{:S(2)}) %copy-start.3) | copy-done | bytes 524312
  5.6 1.0 %copy-done.4 = bf16[128,2048]{1,0:T(8,128)(2,1)S(1)} copy-done((bf16[128,2048]{1,0:T(8,128)(2,1)S(1)}, bf16[128,2048]{1,0:T(8,128)(2,1)}, u32[]{:S(2)}) %copy-start.4) | copy-done | bytes 524312
  6.6 0.9 %copy-done.6 = bf16[2048,64]{0,1:T(8,128)(2,1)S(1)} copy-done((bf16[2048,64]{0,1:T(8,128)(2,1)S(1)}, bf16[2048,64]{0,1:T(8,128)(2,1)}, u32[]{:S(2)}) %copy-start.6) | copy-done | bytes 262168
  7.6 0.9 %copy-done.7 = bf16[2048,64]{0,1:T(8,128)(2,1)S(1)} copy-done((bf16[2048,64]{0,1:T(8,128)(2,1)S(1)}, bf16[2048,64]{0,1:T(8,128)(2,1)}, u32[]{:S(2)}) %copy-start.7) | copy-done | bytes 262168
  8.5 0.9 %copy-done.8 = bf16[512,256]{1,0:T(8,128)(2,1)S(1)} copy-done((bf16[512,256]{1,0:T(8,128)(2,1)S(1)}, bf16[512,256]{1,0:T(8,128)(2,1)}, u32[]{:S(2)}) %copy-start.8) | copy-done | bytes 262168
  9.5 0.6 %prepare.1 = (bf16[256,2048]{1,0:T(8,128)(2,1)S(1)}, bf16[256,2048]{1,0:T(8,128)(2,1)S(1)}, bf16[2048,256]{1,0:T(8,128)(2,1)S(1)}, bf16[1024,256]{1,0:T(8,128)(2...) custom-call(bf16[64,2048]{1,0:T(8,128)(2,1)S(1)} %bitcast.10, ...), custom_call_target="tpu_custom_call" | custom-call | flops 268435456 | bytes 8388608 | tf_op jit(solution)/shard_map/prepare/pallas_call | solution.py:32
  10.7 3.6 %collective-permute-start.2 = (bf16[256,256]{1,0:T(8,128)(2,1)S(1)}, bf16[256,256]{1,0:T(8,128)(2,1)S(1)}, u32[]{:S(2)}, u32[]{:S(2)}) collective-permute-start(bf16[256,256]{1,0:T(8,128)(2,1)S(1)} %copy-done.9), channel_id=1, source_target_pairs={{0,6},{1,7},{2,4},{3,5},{4,2},{5,3},{6,0},{7,1},{8,14},{9,15},{10,... | collective-permute-start | bytes 393224 | tf_op jit(solution)/shard_map/ppermute | solution.py:25
  14.9 3.6 %collective-permute-done.2.refs_3_ = bf16[256,256]{1,0:T(8,128)(2,1)S(1)} collective-permute-done((bf16[256,256]{1,0:T(8,128)(2,1)S(1)}, bf16[256,256]{1,0:T(8,128)(2,1)S(1)}, u32[]{:S(2)}, u32[]{:S(2)}) %collective-permute-start.2) | collective-permute-done | bytes 131104 | tf_op jit(solution)/shard_map/ppermute | solution.py:25
  18.5 2.6 %collective-permute-done.1.refs_2_ = bf16[256,256]{1,0:T(8,128)(2,1)S(1)} collective-permute-done((bf16[256,256]{1,0:T(8,128)(2,1)S(1)}, bf16[256,256]{1,0:T(8,128)(2,1)S(1)}, u32[]{:S(2)}, u32[]{:S(2)}) %collective-permute-start.1) | collective-permute-done | bytes 131104 | tf_op jit(solution)/shard_map/ppermute | solution.py:25
  21.6 0.8 %collective-permute-done.5.refs_6_ = bf16[256,256]{1,0:T(8,128)(2,1)S(1)} collective-permute-done((bf16[256,256]{1,0:T(8,128)(2,1)S(1)}, bf16[256,256]{1,0:T(8,128)(2,1)S(1)}, u32[]{:S(2)}, u32[]{:S(2)}) %collective-permute-start.5) | collective-permute-done | bytes 131104 | tf_op jit(solution)/shard_map/ppermute | solution.py:25
  22.8 1.1 %project_first.1 = (bf16[256,2048]{1,0:T(8,128)(2,1)S(1)}, f32[256,128]{1,0:T(8,128)S(1)}, bf16[152,128]{1,0:T(8,128)(2,1)S(1)}, bf16[256,128]{1,0:T(8,128)(2,1)S(1)}) custom-call(bf16[256,256]{1,0:T(8,128)(2,1)S(1)} %copy-done.9, bf16[256,256]{1,0:T(8,128)(2,1)S(1)} %collective-permute-done.refs_1_, bf16[256,256]{1,0:T(8,128)(2,1)S(1)} %collective-permute-done.1.refs_2_, ...), custom_call_target="tpu_custom_call" | custom-call | flops 536870912 | bytes 2097152 | tf_op jit(solution)/shard_map/project_first/pallas_call | solution.py:32
  23.9 3.7 %collective-permute-start.9 = (bf16[152,128]{1,0:T(8,128)(2,1)S(1)}, bf16[152,128]{1,0:T(8,128)(2,1)S(1)}, u32[]{:S(2)}, u32[]{:S(2)}) collective-permute-start(bf16[152,128]{1,0:T(8,128)(2,1)S(1)} %get-tuple-element.28), channel_id=1, source_target_pairs={{0,24},{8,16},{16,8},{24,0},{1,25},{9,17},{17,9},{25,1},{2,26},{10... | collective-permute-start | bytes 116744 | tf_op jit(solution)/shard_map/ppermute | solution.py:25
  27.6 0.7 %collective-permute-start.7 = (bf16[152,128]{1,0:T(8,128)(2,1)S(1)}, bf16[152,128]{1,0:T(8,128)(2,1)S(1)}, u32[]{:S(2)}, u32[]{:S(2)}) collective-permute-start(bf16[152,128]{1,0:T(8,128)(2,1)S(1)} %get-tuple-element.28), channel_id=1, source_target_pairs={{0,8},{8,0},{16,24},{24,16},{1,9},{9,1},{17,25},{25,17},{2,10},{10... | collective-permute-start | bytes 116744 | tf_op jit(solution)/shard_map/ppermute | solution.py:25
  28.3 1.4 %collective-permute-done.9 = bf16[152,128]{1,0:T(8,128)(2,1)S(1)} collective-permute-done((bf16[152,128]{1,0:T(8,128)(2,1)S(1)}, bf16[152,128]{1,0:T(8,128)(2,1)S(1)}, u32[]{:S(2)}, u32[]{:S(2)}) %collective-permute-start.9) | collective-permute-done | bytes 38944 | tf_op jit(solution)/shard_map/ppermute | solution.py:25
  29.7 2.8 %collective-permute-done.8 = bf16[152,128]{1,0:T(8,128)(2,1)S(1)} collective-permute-done((bf16[152,128]{1,0:T(8,128)(2,1)S(1)}, bf16[152,128]{1,0:T(8,128)(2,1)S(1)}, u32[]{:S(2)}, u32[]{:S(2)}) %collective-permute-start.8) | collective-permute-done | bytes 38944 | tf_op jit(solution)/shard_map/ppermute | solution.py:25
  32.5 1.8 %collective-permute-start.12 = (bf16[4,152,128]{2,1,0:T(8,128)(2,1)S(1)}, bf16[4,152,128]{2,1,0:T(8,128)(2,1)S(1)}, u32[]{:S(2)}, u32[]{:S(2)}) collective-permute-start(bf16[4,152,128]{2,1,0:T(8,128)(2,1)S(1)} %pad_maximum_fusion.refs_0_), channel_id=1, source_target_pairs={{0,6},{1,7},{2,4},{3,5},{4,2},{5,3},{6,0},{7,1},{8,14},{9,15},{10,... | collective-permute-start | bytes 466952 | tf_op jit(solution)/shard_map/ppermute | solution.py:25
  34.3 1.2 %collective-permute-start.11 = (bf16[4,152,128]{2,1,0:T(8,128)(2,1)S(1)}, bf16[4,152,128]{2,1,0:T(8,128)(2,1)S(1)}, u32[]{:S(2)}, u32[]{:S(2)}) collective-permute-start(bf16[4,152,128]{2,1,0:T(8,128)(2,1)S(1)} %pad_maximum_fusion.refs_0_), channel_id=1, source_target_pairs={{0,4},{1,5},{2,6},{3,7},{4,0},{5,1},{6,2},{7,3},{8,12},{9,13},{10,... | collective-permute-start | bytes 466952 | tf_op jit(solution)/shard_map/ppermute | solution.py:25
  36.1 4.2 %collective-permute-done.12.refs_3_ = bf16[4,152,128]{2,1,0:T(8,128)(2,1)S(1)} collective-permute-done((bf16[4,152,128]{2,1,0:T(8,128)(2,1)S(1)}, bf16[4,152,128]{2,1,0:T(8,128)(2,1)S(1)}, u32[]{:S(2)}, u32[]{:S(2)}) %collective-permute-start.12) | collective-permute-done | bytes 155680 | tf_op jit(solution)/shard_map/ppermute | solution.py:25
  40.3 1.8 %collective-permute-done.11.refs_2_ = bf16[4,152,128]{2,1,0:T(8,128)(2,1)S(1)} collective-permute-done((bf16[4,152,128]{2,1,0:T(8,128)(2,1)S(1)}, bf16[4,152,128]{2,1,0:T(8,128)(2,1)S(1)}, u32[]{:S(2)}, u32[]{:S(2)}) %collective-permute-start.11) | collective-permute-done | bytes 155680 | tf_op jit(solution)/shard_map/ppermute | solution.py:25
  42.6 0.8 %project_second.1 = (bf16[2,256,256]{2,1,0:T(8,128)(2,1)S(1)}, f32[256,128]{1,0:T(8,128)S(1)}) custom-call(bf16[256,2048]{1,0:T(8,128)(2,1)S(1)} %get-tuple-element.32.scaled_ref, f32[256,128]{1,0:T(8,128)S(1)} %get-tuple-element.33.inv_ref, bf16[256,2048]{1,0:T(8,128)(2,1)S(1)} %get-tuple-element.34.query_w_ref, bf16[2048,128]{1,0:T(8,128)(2,1)S(1)} %copy-done.5, ...), custom_call_target="tpu_custom_call" | custom-call | flops 402653184 | bytes 2097152 | tf_op jit(solution)/shard_map/project_second/pallas_call | solution.py:32
  43.7 0.7 %copy-done.12 = bf16[3,128]{1,0:T(4,128)(2,1)S(1)} copy-done((bf16[3,128]{1,0:T(4,128)(2,1)S(1)}, bf16[3,128]{1,0:T(4,128)(2,1)}, u32[]{:S(2)}) %copy-start.12) | copy-done | bytes 792
  44.4 2.4 %attend.1 = (bf16[128,256]{1,0:T(8,128)(2,1)S(1)}, bf16[128,256]{1,0:T(8,128)(2,1)S(1)}, f32[1,256]{1,0:T(1,128)}) custom-call(bf16[4,152,128]{2,1,0:T(8,128)(2,1)S(1)} %pad_maximum_fusion.refs_0_, bf16[4,152,128]{2,1,0:T(8,128)(2,1)S(1)} %collective-permute-done.10.refs_1_, bf16[4,152,128]{2,1,0:T(8,128)(2,1)S(1)} %collective-permute-done.11.refs_2_, ...), custom_call_target="tpu_custom_call" | custom-call | flops 1073741824 | bytes 4194304 | tf_op jit(solution)/shard_map/attend/pallas_call | solution.py:32
  47.1 1.0 %collective-permute-done.17.got_ref = bf16[128,256]{1,0:T(8,128)(2,1)S(1)} collective-permute-done((bf16[128,256]{1,0:T(8,128)(2,1)S(1)}, bf16[128,256]{1,0:T(8,128)(2,1)S(1)}, u32[]{:S(2)}, u32[]{:S(2)}) %collective-permute-start.17) | collective-permute-done | bytes 65568 | tf_op jit(solution)/shard_map/ppermute | solution.py:25
  48.5 1.8 %collective-permute-start.19 = (bf16[32,2048]{1,0:T(8,128)(2,1)S(1)}, bf16[32,2048]{1,0:T(8,128)(2,1)S(1)}, u32[]{:S(2)}, u32[]{:S(2)}) collective-permute-start(bf16[32,2048]{1,0:T(8,128)(2,1)S(1)} %get-tuple-element.42), channel_id=1, source_target_pairs={{0,6},{1,7},{2,4},{3,5},{4,2},{5,3},{6,0},{7,1},{8,14},{9,15},{10,... | collective-permute-start | bytes 393224 | tf_op jit(solution)/shard_map/ppermute | solution.py:25
  50.3 1.2 %collective-permute-start.20 = (bf16[32,2048]{1,0:T(8,128)(2,1)S(1)}, bf16[32,2048]{1,0:T(8,128)(2,1)S(1)}, u32[]{:S(2)}, u32[]{:S(2)}) collective-permute-start(bf16[32,2048]{1,0:T(8,128)(2,1)S(1)} %get-tuple-element.43), channel_id=1, source_target_pairs={{0,4},{1,5},{2,6},{3,7},{4,0},{5,1},{6,2},{7,3},{8,12},{9,13},{10,... | collective-permute-start | bytes 393224 | tf_op jit(solution)/shard_map/ppermute | solution.py:25
  52.1 3.8 %collective-permute-done.19 = bf16[32,2048]{1,0:T(8,128)(2,1)S(1)} collective-permute-done((bf16[32,2048]{1,0:T(8,128)(2,1)S(1)}, bf16[32,2048]{1,0:T(8,128)(2,1)S(1)}, u32[]{:S(2)}, u32[]{:S(2)}) %collective-permute-start.19) | collective-permute-done | bytes 131104 | tf_op jit(solution)/shard_map/ppermute | solution.py:25
  55.9 2.1 %collective-permute-done.20 = bf16[32,2048]{1,0:T(8,128)(2,1)S(1)} collective-permute-done((bf16[32,2048]{1,0:T(8,128)(2,1)S(1)}, bf16[32,2048]{1,0:T(8,128)(2,1)S(1)}, u32[]{:S(2)}, u32[]{:S(2)}) %collective-permute-start.20) | collective-permute-done | bytes 131104 | tf_op jit(solution)/shard_map/ppermute | solution.py:25
  58.1 0.7 %add_convert_fusion = bf16[32,2048]{1,0:T(8,128)(2,1)} fusion(bf16[32,2048]{1,0:T(8,128)(2,1)S(1)} %collective-permute-done.21, bf16[32,2048]{1,0:T(8,128)(2,1)S(1)} %collective-permute-done.20, f32[32,2048]{1,0:T(8,128)S(1)} %get-tuple-element.41, bf16[32,2048]{1,0:T(8,128)(2,1)S(1)} %collective-permute-done.19), kind=kLoop, calls=%fused_computation | loop fusion | flops 458752 | bytes 786432 | tf_op jit(solution)/shard_map/convert_element_type | solution.py:388
  (45 shorter events, 4.7 us)
Async XLA Ops:
  1.3 1.1 %copy-start = (bf16[2048,192]{0,1:T(8,128)(2,1)S(1)}, bf16[2048,192]{0,1:T(8,128)(2,1)}, u32[]{:S(2)}) copy-start(bf16[2048,192]{0,1:T(8,128)(2,1)} %param.15) | copy-start | bytes 2359300
  2.5 1.0 %copy-start.1 = (bf16[2048,128]{1,0:T(8,128)(2,1)S(1)}, bf16[2048,128]{1,0:T(8,128)(2,1)}, u32[]{:S(2)}) copy-start(bf16[2048,128]{1,0:T(8,128)(2,1)} %pre_ref.1) | copy-start | bytes 1572868
  3.5 1.0 %copy-start.2 = (bf16[2048,128]{1,0:T(8,128)(2,1)S(1)}, bf16[2048,128]{1,0:T(8,128)(2,1)}, u32[]{:S(2)}) copy-start(bf16[2048,128]{1,0:T(8,128)(2,1)} %value_ref.1) | copy-start | bytes 1572868
  4.5 1.0 %copy-start.3 = (bf16[128,2048]{1,0:T(8,128)(2,1)S(1)}, bf16[128,2048]{1,0:T(8,128)(2,1)}, u32[]{:S(2)}) copy-start(bf16[128,2048]{1,0:T(8,128)(2,1)} %attend_ref.1) | copy-start | bytes 1572868
  5.6 1.0 %copy-start.4 = (bf16[128,2048]{1,0:T(8,128)(2,1)S(1)}, bf16[128,2048]{1,0:T(8,128)(2,1)}, u32[]{:S(2)}) copy-start(bf16[128,2048]{1,0:T(8,128)(2,1)} %conv_ref.1) | copy-start | bytes 1572868
  6.6 0.9 %copy-start.6 = (bf16[2048,64]{0,1:T(8,128)(2,1)S(1)}, bf16[2048,64]{0,1:T(8,128)(2,1)}, u32[]{:S(2)}) copy-start(bf16[2048,64]{0,1:T(8,128)(2,1)} %param.16) | copy-start | bytes 786436
  7.6 0.9 %copy-start.7 = (bf16[2048,64]{0,1:T(8,128)(2,1)S(1)}, bf16[2048,64]{0,1:T(8,128)(2,1)}, u32[]{:S(2)}) copy-start(bf16[2048,64]{0,1:T(8,128)(2,1)} %param.17) | copy-start | bytes 786436
  9.5 1.2 %copy-start.9 = (bf16[256,256]{1,0:T(8,128)(2,1)S(1)}, bf16[256,256]{1,0:T(8,128)(2,1)}, u32[]{:S(2)}) copy-start(bf16[256,256]{1,0:T(8,128)(2,1)} %refs_0_.1) | copy-start | bytes 393220
  10.1 12.6 %copy-start.10 = (f32[2048]{0:T(1024)S(1)}, f32[2048]{0:T(1024)}, u32[]{:S(2)}) copy-start(f32[2048]{0:T(1024)} %param.14) | copy-start | bytes 24580
  10.1 37.9 %collective-permute-start.18 = (bf16[256,2048]{1,0:T(8,128)(2,1)S(1)}, bf16[256,2048]{1,0:T(8,128)(2,1)S(1)}, u32[]{:S(2)}, u32[]{:S(2)}) collective-permute-start(bf16[256,2048]{1,0:T(8,128)(2,1)S(1)} %get-tuple-element.40.own_w_ref), channel_id=1, source_target_pairs={{0,1},{1,0},{2,3},{3,2},{4,5},{5,4},{6,7},{7,6},{8,9},{9,8},{10,11... | collective-permute-start | bytes 3145736 | tf_op jit(solution)/shard_map/ppermute | solution.py:25
  10.7 7.8 %collective-permute-start.2 = (bf16[256,256]{1,0:T(8,128)(2,1)S(1)}, bf16[256,256]{1,0:T(8,128)(2,1)S(1)}, u32[]{:S(2)}, u32[]{:S(2)}) collective-permute-start(bf16[256,256]{1,0:T(8,128)(2,1)S(1)} %copy-done.9), channel_id=1, source_target_pairs={{0,6},{1,7},{2,4},{3,5},{4,2},{5,3},{6,0},{7,1},{8,14},{9,15},{10,... | collective-permute-start | bytes 393224 | tf_op jit(solution)/shard_map/ppermute | solution.py:25
  14.3 6.8 %collective-permute-start.1 = (bf16[256,256]{1,0:T(8,128)(2,1)S(1)}, bf16[256,256]{1,0:T(8,128)(2,1)S(1)}, u32[]{:S(2)}, u32[]{:S(2)}) collective-permute-start(bf16[256,256]{1,0:T(8,128)(2,1)S(1)} %copy-done.9), channel_id=1, source_target_pairs={{0,4},{1,5},{2,6},{3,7},{4,0},{5,1},{6,2},{7,3},{8,12},{9,13},{10,... | collective-permute-start | bytes 393224 | tf_op jit(solution)/shard_map/ppermute | solution.py:25
  14.8 6.6 %collective-permute-start = (bf16[256,256]{1,0:T(8,128)(2,1)S(1)}, bf16[256,256]{1,0:T(8,128)(2,1)S(1)}, u32[]{:S(2)}, u32[]{:S(2)}) collective-permute-start(bf16[256,256]{1,0:T(8,128)(2,1)S(1)} %copy-done.9), channel_id=1, source_target_pairs={{0,2},{1,3},{2,0},{3,1},{4,6},{5,7},{6,4},{7,5},{8,10},{9,11},{10,... | collective-permute-start | bytes 393224 | tf_op jit(solution)/shard_map/ppermute | solution.py:25
  14.9 6.8 %collective-permute-start.3 = (bf16[256,256]{1,0:T(8,128)(2,1)S(1)}, bf16[256,256]{1,0:T(8,128)(2,1)S(1)}, u32[]{:S(2)}, u32[]{:S(2)}) collective-permute-start(bf16[256,256]{1,0:T(8,128)(2,1)S(1)} %copy-done.9), channel_id=1, source_target_pairs={{0,1},{1,0},{2,3},{3,2},{4,5},{5,4},{6,7},{7,6},{8,9},{9,8},{10,11... | collective-permute-start | bytes 393224 | tf_op jit(solution)/shard_map/ppermute | solution.py:25
  18.5 3.2 %collective-permute-start.6 = (bf16[256,256]{1,0:T(8,128)(2,1)S(1)}, bf16[256,256]{1,0:T(8,128)(2,1)S(1)}, u32[]{:S(2)}, u32[]{:S(2)}) collective-permute-start(bf16[256,256]{1,0:T(8,128)(2,1)S(1)} %collective-permute-done.2.refs_3_), channel_id=1, source_target_pairs={{0,1},{1,0},{2,3},{3,2},{4,5},{5,4},{6,7},{7,6},{8,9},{9,8},{10,11... | collective-permute-start | bytes 393224 | tf_op jit(solution)/shard_map/ppermute | solution.py:25
  21.1 1.3 %collective-permute-start.5 = (bf16[256,256]{1,0:T(8,128)(2,1)S(1)}, bf16[256,256]{1,0:T(8,128)(2,1)S(1)}, u32[]{:S(2)}, u32[]{:S(2)}) collective-permute-start(bf16[256,256]{1,0:T(8,128)(2,1)S(1)} %collective-permute-done.1.refs_2_), channel_id=1, source_target_pairs={{0,1},{1,0},{2,3},{3,2},{4,5},{5,4},{6,7},{7,6},{8,9},{9,8},{10,11... | collective-permute-start | bytes 393224 | tf_op jit(solution)/shard_map/ppermute | solution.py:25
  21.4 1.3 %collective-permute-start.4 = (bf16[256,256]{1,0:T(8,128)(2,1)S(1)}, bf16[256,256]{1,0:T(8,128)(2,1)S(1)}, u32[]{:S(2)}, u32[]{:S(2)}) collective-permute-start(bf16[256,256]{1,0:T(8,128)(2,1)S(1)} %collective-permute-done.refs_1_), channel_id=1, source_target_pairs={{0,1},{1,0},{2,3},{3,2},{4,5},{5,4},{6,7},{7,6},{8,9},{9,8},{10,11... | collective-permute-start | bytes 393224 | tf_op jit(solution)/shard_map/ppermute | solution.py:25
  22.8 19.8 %copy-start.5 = (bf16[2048,128]{1,0:T(8,128)(2,1)S(1)}, bf16[2048,128]{1,0:T(8,128)(2,1)}, u32[]{:S(2)}) copy-start(bf16[2048,128]{1,0:T(8,128)(2,1)} %gate_w_ref.1) | copy-start | bytes 1572868
  23.9 5.8 %collective-permute-start.9 = (bf16[152,128]{1,0:T(8,128)(2,1)S(1)}, bf16[152,128]{1,0:T(8,128)(2,1)S(1)}, u32[]{:S(2)}, u32[]{:S(2)}) collective-permute-start(bf16[152,128]{1,0:T(8,128)(2,1)S(1)} %get-tuple-element.28), channel_id=1, source_target_pairs={{0,24},{8,16},{16,8},{24,0},{1,25},{9,17},{17,9},{25,1},{2,26},{10... | collective-permute-start | bytes 116744 | tf_op jit(solution)/shard_map/ppermute | solution.py:25
  27.6 4.9 %collective-permute-start.8 = (bf16[152,128]{1,0:T(8,128)(2,1)S(1)}, bf16[152,128]{1,0:T(8,128)(2,1)S(1)}, u32[]{:S(2)}, u32[]{:S(2)}) collective-permute-start(bf16[152,128]{1,0:T(8,128)(2,1)S(1)} %get-tuple-element.28), channel_id=1, source_target_pairs={{0,16},{8,24},{16,0},{24,8},{1,17},{9,25},{17,1},{25,9},{2,18},{10... | collective-permute-start | bytes 116744 | tf_op jit(solution)/shard_map/ppermute | solution.py:25
  27.6 4.9 %collective-permute-start.7 = (bf16[152,128]{1,0:T(8,128)(2,1)S(1)}, bf16[152,128]{1,0:T(8,128)(2,1)S(1)}, u32[]{:S(2)}, u32[]{:S(2)}) collective-permute-start(bf16[152,128]{1,0:T(8,128)(2,1)S(1)} %get-tuple-element.28), channel_id=1, source_target_pairs={{0,8},{8,0},{16,24},{24,16},{1,9},{9,1},{17,25},{25,17},{2,10},{10... | collective-permute-start | bytes 116744 | tf_op jit(solution)/shard_map/ppermute | solution.py:25
  32.5 7.8 %collective-permute-start.12 = (bf16[4,152,128]{2,1,0:T(8,128)(2,1)S(1)}, bf16[4,152,128]{2,1,0:T(8,128)(2,1)S(1)}, u32[]{:S(2)}, u32[]{:S(2)}) collective-permute-start(bf16[4,152,128]{2,1,0:T(8,128)(2,1)S(1)} %pad_maximum_fusion.refs_0_), channel_id=1, source_target_pairs={{0,6},{1,7},{2,4},{3,5},{4,2},{5,3},{6,0},{7,1},{8,14},{9,15},{10,... | collective-permute-start | bytes 466952 | tf_op jit(solution)/shard_map/ppermute | solution.py:25
  34.3 7.7 %collective-permute-start.11 = (bf16[4,152,128]{2,1,0:T(8,128)(2,1)S(1)}, bf16[4,152,128]{2,1,0:T(8,128)(2,1)S(1)}, u32[]{:S(2)}, u32[]{:S(2)}) collective-permute-start(bf16[4,152,128]{2,1,0:T(8,128)(2,1)S(1)} %pad_maximum_fusion.refs_0_), channel_id=1, source_target_pairs={{0,4},{1,5},{2,6},{3,7},{4,0},{5,1},{6,2},{7,3},{8,12},{9,13},{10,... | collective-permute-start | bytes 466952 | tf_op jit(solution)/shard_map/ppermute | solution.py:25
  35.5 6.6 %collective-permute-start.10 = (bf16[4,152,128]{2,1,0:T(8,128)(2,1)S(1)}, bf16[4,152,128]{2,1,0:T(8,128)(2,1)S(1)}, u32[]{:S(2)}, u32[]{:S(2)}) collective-permute-start(bf16[4,152,128]{2,1,0:T(8,128)(2,1)S(1)} %pad_maximum_fusion.refs_0_), channel_id=1, source_target_pairs={{0,2},{1,3},{2,0},{3,1},{4,6},{5,7},{6,4},{7,5},{8,10},{9,11},{10,... | collective-permute-start | bytes 466952 | tf_op jit(solution)/shard_map/ppermute | solution.py:25
  36.1 7.4 %collective-permute-start.13 = (bf16[4,152,128]{2,1,0:T(8,128)(2,1)S(1)}, bf16[4,152,128]{2,1,0:T(8,128)(2,1)S(1)}, u32[]{:S(2)}, u32[]{:S(2)}) collective-permute-start(bf16[4,152,128]{2,1,0:T(8,128)(2,1)S(1)} %pad_maximum_fusion.refs_0_), channel_id=1, source_target_pairs={{0,1},{1,0},{2,3},{3,2},{4,5},{5,4},{6,7},{7,6},{8,9},{9,8},{10,11... | collective-permute-start | bytes 466952 | tf_op jit(solution)/shard_map/ppermute | solution.py:25
  40.3 3.1 %collective-permute-start.16 = (bf16[4,152,128]{2,1,0:T(8,128)(2,1)S(1)}, bf16[4,152,128]{2,1,0:T(8,128)(2,1)S(1)}, u32[]{:S(2)}, u32[]{:S(2)}) collective-permute-start(bf16[4,152,128]{2,1,0:T(8,128)(2,1)S(1)} %collective-permute-done.12.refs_3_), channel_id=1, source_target_pairs={{0,1},{1,0},{2,3},{3,2},{4,5},{5,4},{6,7},{7,6},{8,9},{9,8},{10,11... | collective-permute-start | bytes 466952 | tf_op jit(solution)/shard_map/ppermute | solution.py:25
  42.1 1.4 %collective-permute-start.15 = (bf16[4,152,128]{2,1,0:T(8,128)(2,1)S(1)}, bf16[4,152,128]{2,1,0:T(8,128)(2,1)S(1)}, u32[]{:S(2)}, u32[]{:S(2)}) collective-permute-start(bf16[4,152,128]{2,1,0:T(8,128)(2,1)S(1)} %collective-permute-done.11.refs_2_), channel_id=1, source_target_pairs={{0,1},{1,0},{2,3},{3,2},{4,5},{5,4},{6,7},{7,6},{8,9},{9,8},{10,11... | collective-permute-start | bytes 466952 | tf_op jit(solution)/shard_map/ppermute | solution.py:25
  42.1 1.5 %collective-permute-start.14 = (bf16[4,152,128]{2,1,0:T(8,128)(2,1)S(1)}, bf16[4,152,128]{2,1,0:T(8,128)(2,1)S(1)}, u32[]{:S(2)}, u32[]{:S(2)}) collective-permute-start(bf16[4,152,128]{2,1,0:T(8,128)(2,1)S(1)} %collective-permute-done.10.refs_1_), channel_id=1, source_target_pairs={{0,1},{1,0},{2,3},{3,2},{4,5},{5,4},{6,7},{7,6},{8,9},{9,8},{10,11... | collective-permute-start | bytes 466952 | tf_op jit(solution)/shard_map/ppermute | solution.py:25
  46.8 1.3 %collective-permute-start.17 = (bf16[128,256]{1,0:T(8,128)(2,1)S(1)}, bf16[128,256]{1,0:T(8,128)(2,1)S(1)}, u32[]{:S(2)}, u32[]{:S(2)}) collective-permute-start(bf16[128,256]{1,0:T(8,128)(2,1)S(1)} %get-tuple-element.39), channel_id=1, source_target_pairs={{0,1},{1,0},{2,3},{3,2},{4,5},{5,4},{6,7},{7,6},{8,9},{9,8},{10,11... | collective-permute-start | bytes 196616 | tf_op jit(solution)/shard_map/ppermute | solution.py:25
  48.5 7.3 %collective-permute-start.19 = (bf16[32,2048]{1,0:T(8,128)(2,1)S(1)}, bf16[32,2048]{1,0:T(8,128)(2,1)S(1)}, u32[]{:S(2)}, u32[]{:S(2)}) collective-permute-start(bf16[32,2048]{1,0:T(8,128)(2,1)S(1)} %get-tuple-element.42), channel_id=1, source_target_pairs={{0,6},{1,7},{2,4},{3,5},{4,2},{5,3},{6,0},{7,1},{8,14},{9,15},{10,... | collective-permute-start | bytes 393224 | tf_op jit(solution)/shard_map/ppermute | solution.py:25
  50.3 7.7 %collective-permute-start.20 = (bf16[32,2048]{1,0:T(8,128)(2,1)S(1)}, bf16[32,2048]{1,0:T(8,128)(2,1)S(1)}, u32[]{:S(2)}, u32[]{:S(2)}) collective-permute-start(bf16[32,2048]{1,0:T(8,128)(2,1)S(1)} %get-tuple-element.43), channel_id=1, source_target_pairs={{0,4},{1,5},{2,6},{3,7},{4,0},{5,1},{6,2},{7,3},{8,12},{9,13},{10,... | collective-permute-start | bytes 393224 | tf_op jit(solution)/shard_map/ppermute | solution.py:25
  51.5 6.5 %collective-permute-start.21 = (bf16[32,2048]{1,0:T(8,128)(2,1)S(1)}, bf16[32,2048]{1,0:T(8,128)(2,1)S(1)}, u32[]{:S(2)}, u32[]{:S(2)}) collective-permute-start(bf16[32,2048]{1,0:T(8,128)(2,1)S(1)} %get-tuple-element.44), channel_id=1, source_target_pairs={{0,2},{1,3},{2,0},{3,1},{4,6},{5,7},{6,4},{7,5},{8,10},{9,11},{10,... | collective-permute-start | bytes 393224 | tf_op jit(solution)/shard_map/ppermute | solution.py:25
  (3 other events, 2.3 us)
